TPU v7x, 256 devices: a 4x2x16 block of a 4x16x16 slice. The times are simulated.
256 devices in a mesh: grp: 2 (over y), sp: 32 (over z, core), tp: 4 (over x).
Axes of the slice: x: 4, y: 2, z: 16, core: 2. Of those that a mesh axis runs over, the one named last changes fastest.
The devices are a block of a 4x16x16 slice.
Arguments:
- recept: bfloat16 [32768, 2048], P(('grp', 'sp'), 'tp'), parts along dimension 0, may hold values from -6 to 6
- key_input: bfloat16 [32768, 2048], P(('grp', 'sp'), 'tp'), parts along dimension 0, may hold values from -6 to 6
- value_input: bfloat16 [32768, 2048], P(('grp', 'sp'), 'tp'), parts along dimension 0, may hold values from -6 to 6
- output_gate_input: bfloat16 [32768, 2048], P(('grp', 'sp'), 'tp'), parts along dimension 0, may hold values from -6 to 6
- decay_input_part: bfloat16 [32768, 2048], P(('grp', 'sp'), 'tp'), parts along dimension 0, may hold values from -4.8 to 4.8
- correction_rate_input: bfloat16 [32768, 2048], P(('grp', 'sp'), 'tp'), parts along dimension 0, may hold values from -4 to 4
- head_decay_offset: float32 [32768, 32], P(('grp', 'sp'), 'tp'), parts along dimension 0, may hold values from -2.1 to 0
- decay_fixed_bias: float32 [2048], P('tp'), may hold values from -11.5 to -2.8
- correction_rate_bias: float32 [2048], P('tp'), may hold values from -8.5 to 1
- head_norm_gain: float32 [2048], P('tp'), may hold values from 0.1 to 1.9
- self_term_weight: float32 [2048], P('tp'), may hold values from -2 to 2
- output_weight_matrix: bfloat16 [2048, 2048], P('tp'), may hold values from -0.125 to 0.125
- residual: bfloat16 [32768, 2048], P(('grp', 'sp', 'tp')), parts along dimension 0, may hold values from -6 to 6
- feedforward_norm_gain: float32 [2048], replicated, may hold values from 0.1 to 1.9
- routed_expert_index: int32 [32768, 2], P(('grp', 'sp', 'tp')), parts along dimension 0, may hold values from 0 to 31, all different within a row; in each aligned block of 128 rows (0 to 127, 128 to 255, ...) at most 12 rows name the same one
- routed_expert_weight: float32 [32768, 2], P(('grp', 'sp', 'tp')), parts along dimension 0, may hold values from 0.2 to 1
- gate_weight_experts: bfloat16 [32, 2048, 1024], P('sp', None, 'tp'), may hold values from -0.125 to 0.125
- up_weight_experts: bfloat16 [32, 2048, 1024], P('sp', None, 'tp'), may hold values from -0.125 to 0.125
- down_weight_experts: bfloat16 [32, 1024, 2048], P('sp', 'tp'), may hold values from -0.1875 to 0.1875
Outputs:
- output: bfloat16 [32768, 2048], P(('grp', 'sp', 'tp')), parts along dimension 0
There are 2 independent parts, one for each index of `grp`. A program takes and returns all parts, laid end to end along the dimension named above; an argument that names none is the same for every part. Nothing has to cross between parts.
Inputs may be any that keep to these rules, and one draw needn't show every extreme that they name: `routed_expert_index`: in each aligned block of 128 rows (the rows of one device) no expert is named by more than 12 routes; the two experts of a row differ.
All inputs are finite; a program needn't handle non-finite values.
Results may differ from a plain program's by a relative error of at most 0.0058.
Values may be sent and summed in bfloat16 or wider, within the bound.
A program may use at most 128 MiB of HBM per device.

v0:
```python
import jax
import jax.numpy as jnp
from jax import lax
from jax.sharding import Mesh
from jax.sharding import PartitionSpec as P

SPAN = 64
SP = ("sp_0", "sp_1")
GRP_SP = ("grp", "sp_0", "sp_1")
GRP_SP_TP = ("grp", "sp_0", "sp_1", "tp")


PRECISE = lax.Precision.HIGHEST
GROUP_EPS = 0.00064
NORM_EPS = 1e-06


def neutral_like(shard, identity):
    return jax.tree.map(
        lambda part, zero: jnp.zeros_like(part) + jnp.asarray(zero, part.dtype), shard, identity
    )


def prefix_by_axis(shard, axes, combine, identity):
    before = start = neutral_like(shard, identity)
    so_far = shard
    for axis in reversed(axes):
        length, mine = (lax.axis_size(axis), lax.axis_index(axis))
        pieces = jax.tree.map(lambda part: lax.all_gather(part, axis), so_far)
        inside, so_far = (start, start)
        for k in range(length):
            passed = k < mine
            so_far = combine(so_far, jax.tree.map(lambda part: part[k], pieces))
            inside = jax.tree.map(lambda new, old: jnp.where(passed, new, old), so_far, inside)
        before = combine(inside, before)
    return before


def split_up(shard, dim, length):
    before, after = (shard.shape[:dim], shard.shape[dim + 1 :])
    return jnp.moveaxis(shard.reshape(*before, length, -1, *after), dim, 0)


def summed_on_arrival(shard, axis, dim):
    parts = split_up(shard, dim, lax.axis_size(axis))
    arrived = lax.all_to_all(parts, axis, split_axis=0, concat_axis=0, tiled=True)
    return arrived.sum(axis=0)


def sent_and_summed(shard, axis, dim):
    parts = split_up(shard, dim, lax.axis_size(axis))
    arrived = lax.all_to_all(parts, axis, split_axis=0, concat_axis=0, tiled=True)
    return arrived.astype(jnp.float32).sum(axis=0)


def exchange_in_groups(shard, axis, split_dim, concat_dim, work, item_dim, out_dim):
    items = jax.tree.leaves(shard)[0].shape[item_dim]
    count = 2 if items % 2 == 0 else 1
    gathered = []
    for k in range(count):
        group = jax.tree.map(
            lambda a: lax.slice_in_dim(
                a, k * (items // count), (k + 1) * (items // count), axis=item_dim
            ),
            shard,
        )
        gathered.append(
            work(
                lax.all_to_all(
                    group, axis, split_axis=split_dim, concat_axis=concat_dim, tiled=True
                )
            )
        )
    return jax.tree.map(lambda *parts: jnp.concatenate(parts, axis=out_dim), *gathered)


def chain_combine(earlier, later):
    transit = jnp.einsum("hij,hjk->hik", earlier[0], later[0], precision=PRECISE)
    carried = jnp.einsum("hij,hjk->hik", earlier[1], later[0], precision=PRECISE) + later[1]
    return (transit, carried)


def pair_scores(left, right):
    return jnp.einsum("bhtn,bhsn->bhts", left, right, precision=PRECISE)


def apply_scores(left, right):
    return jnp.einsum("bhts,bhsn->bhtn", left, right, precision=PRECISE)


def outer_sum(left, right):
    return jnp.einsum("bhtn,bhtm->bhnm", left, right, precision=PRECISE)


def square_blocks(left, right):
    return jnp.einsum("bhts,bhsu->bhtu", left, right, precision=PRECISE)


def unit_lower_inverse(strict_lower, span):
    inverse = jnp.eye(span, dtype=jnp.float32) + strict_lower
    power = strict_lower
    for level in range(1, (span - 1).bit_length()):
        power = square_blocks(power, power)
        inverse = inverse + square_blocks(power, inverse)
    return inverse


def mixer(
    recept,
    key_input,
    value_input,
    output_gate_input,
    decay_input_part,
    correction_rate_input,
    head_decay_offset,
    decay_fixed_bias,
    correction_rate_bias,
    head_norm_gain,
    self_term_weight,
    span,
):
    sequence_length, channel_width = recept.shape
    head_split = head_decay_offset.shape[1]
    head_width = channel_width // head_split
    blocks = sequence_length // span

    def split_heads(tensor):
        return (
            tensor.astype(jnp.float32)
            .reshape(blocks, span, head_split, head_width)
            .transpose(0, 2, 1, 3)
        )

    weight_logarithm = (
        -jax.nn.softplus(-(decay_fixed_bias + decay_input_part.astype(jnp.float32))) - 0.5
    )
    decay_logarithm = (
        -jnp.exp(weight_logarithm).reshape(sequence_length, head_split, head_width)
        + head_decay_offset[:, :, None]
    )
    decay_logarithm = split_heads(decay_logarithm.reshape(sequence_length, channel_width))
    rate = split_heads(
        jax.nn.sigmoid(correction_rate_bias + correction_rate_input.astype(jnp.float32))
    )
    receptance_per_head, key_per_head, value_per_head = (
        split_heads(recept),
        split_heads(key_input),
        split_heads(value_input),
    )
    unit_key = key_per_head * lax.rsqrt(
        jnp.sum(key_per_head * key_per_head, axis=-1, keepdims=True) + NORM_EPS
    )
    remove_vec = -unit_key
    write_vec = unit_key * rate
    cumul = jnp.cumsum(decay_logarithm, axis=2)
    remove_til = remove_vec * jnp.exp(cumul - decay_logarithm)
    recept_til = receptance_per_head * jnp.exp(cumul)
    write_hat = write_vec * jnp.exp(-cumul)
    key_hat = key_per_head * jnp.exp(-cumul)
    ending = jnp.exp(cumul[:, :, -1:, :])
    offsets = jnp.arange(span, dtype=jnp.int32)
    strict = offsets[:, None] > offsets[None, :]
    within = offsets[:, None] >= offsets[None, :]
    remove_write = jnp.where(strict, pair_scores(remove_til, write_hat), 0.0)
    remove_key = jnp.where(strict, pair_scores(remove_til, key_hat), 0.0)
    read_write = jnp.where(within, pair_scores(recept_til, write_hat), 0.0)
    read_key = jnp.where(within, pair_scores(recept_til, key_hat), 0.0)
    inverse = unit_lower_inverse(remove_write, span)
    inv_remove = apply_scores(inverse, remove_til)
    inv_value = apply_scores(inverse, apply_scores(remove_key, value_per_head))
    read_map = recept_til + apply_scores(read_write, inv_remove)
    read_own = apply_scores(read_write, inv_value) + apply_scores(read_key, value_per_head)
    write_end = write_hat * ending
    key_end = key_hat * ending
    eye_head = jnp.eye(head_width, dtype=jnp.float32)
    transit = outer_sum(inv_remove, write_end) + eye_head * ending[:, :, 0, None, :]
    added = outer_sum(inv_value, write_end) + outer_sum(value_per_head, key_end)
    identity = jnp.broadcast_to(eye_head, (head_split, head_width, head_width))
    zero_state = jnp.zeros((head_split, head_width, head_width), jnp.float32)

    def block_step(carry, inputs):
        return (chain_combine(carry, inputs), carry)

    device_total, block_starts = lax.scan(block_step, (identity, zero_state), (transit, added))
    prefix = prefix_by_axis(device_total, SP, chain_combine, (identity, zero_state))
    entering = prefix[1]
    true_start = (
        jnp.einsum("hvk,bhkm->bhvm", entering, block_starts[0], precision=PRECISE) + block_starts[1]
    )
    readout = jnp.einsum("bhtk,bhvk->bhtv", read_map, true_start, precision=PRECISE) + read_own
    center = jnp.mean(readout, axis=-1, keepdims=True)
    spread = jnp.mean(jnp.square(readout - center), axis=-1, keepdims=True)
    gains = head_norm_gain.reshape(head_split, head_width)[None, :, None, :]
    normalized_state = (readout - center) * lax.rsqrt(spread + GROUP_EPS) * gains
    self_term_head = self_term_weight.reshape(head_split, head_width)[None, :, None, :]
    self_term = (
        jnp.sum(receptance_per_head * key_per_head * self_term_head, axis=-1, keepdims=True)
        * value_per_head
    )
    merged_heads = (
        (normalized_state + self_term).transpose(0, 2, 1, 3).reshape(sequence_length, channel_width)
    )
    return (merged_heads * output_gate_input.astype(jnp.float32)).astype(jnp.bfloat16)


def local(
    recept,
    key_input,
    value_input,
    output_gate_input,
    decay_input_part,
    correction_rate_input,
    head_decay_offset,
    decay_fixed_bias,
    correction_rate_bias,
    head_norm_gain,
    self_term_weight,
    output_weight_matrix,
    residual,
    feedforward_norm_gain,
    routed_expert_index,
    routed_expert_weight,
    gate_weight_experts,
    up_weight_experts,
    down_weight_experts,
):
    attention_result = mixer(
        recept,
        key_input,
        value_input,
        output_gate_input,
        decay_input_part,
        correction_rate_input,
        head_decay_offset,
        decay_fixed_bias,
        correction_rate_bias,
        head_norm_gain,
        self_term_weight,
        SPAN,
    )
    proj = summed_on_arrival(
        jnp.dot(attention_result, output_weight_matrix, preferred_element_type=jnp.float32), "tp", 0
    )
    proj = proj.astype(jnp.bfloat16)
    stream = residual.astype(jnp.float32) + lax.optimization_barrier(proj).astype(jnp.float32)
    ffn_in = (
        stream
        * lax.rsqrt(jnp.mean(stream * stream, axis=-1, keepdims=True) + NORM_EPS)
        * feedforward_norm_gain
    ).astype(jnp.bfloat16)
    local_rows = ffn_in.shape[0]
    top_count = routed_expert_index.shape[1]
    experts = gate_weight_experts.shape[0] * lax.axis_size(SP)
    capacity = max(2, 3 * local_rows // experts)
    flat_ids = routed_expert_index.reshape(-1)
    hits = (flat_ids[:, None] == jnp.arange(experts, dtype=jnp.int32)[None, :]).astype(jnp.int32)
    earlier_hits = jnp.cumsum(hits, axis=0) - hits
    slot_index = jnp.sum(earlier_hits * hits, axis=1)
    target = flat_ids * capacity + slot_index
    places = (target[:, None] == jnp.arange(experts * capacity, dtype=jnp.int32)[None, :]).astype(
        jnp.bfloat16
    )
    places = jnp.sum(places.reshape(local_rows, top_count, experts * capacity), axis=1)
    outgoing = jnp.einsum("rs,rd->sd", places, ffn_in, preferred_element_type=jnp.float32)
    outgoing = outgoing.astype(jnp.bfloat16).reshape(experts, capacity, ffn_in.shape[1])

    def expert_part(incoming):
        flat = incoming.reshape(-1, incoming.shape[-1])
        gated = jnp.dot(flat, gate_weight_experts[0], preferred_element_type=jnp.float32)
        upward = jnp.dot(flat, up_weight_experts[0], preferred_element_type=jnp.float32)
        hidden = (jax.nn.silu(gated) * upward).astype(jnp.bfloat16)
        result = jnp.dot(hidden, down_weight_experts[0], preferred_element_type=jnp.float32)
        return result.astype(jnp.bfloat16).reshape(incoming.shape)

    def serve_group(incoming):
        spread_rows = lax.optimization_barrier(
            expert_part(lax.all_gather(incoming, "tp", axis=0, tiled=True))
        ).astype(jnp.float32)
        summed = sent_and_summed(spread_rows.astype(jnp.bfloat16), "tp", 0)
        return lax.all_to_all(
            summed.astype(jnp.bfloat16), SP, split_axis=0, concat_axis=0, tiled=True
        )

    expert_out = exchange_in_groups(outgoing, SP, 0, 0, serve_group, 1, 1)
    table = expert_out.reshape(experts * capacity, expert_out.shape[-1])
    fetched = jnp.take(table, target, axis=0).astype(jnp.float32)
    weighted = jnp.sum(
        fetched.reshape(local_rows, top_count, -1) * routed_expert_weight[:, :, None], axis=1
    )
    return (stream + weighted).astype(jnp.bfloat16)


def solution(mesh):
    finer = Mesh(
        mesh.devices.reshape(mesh.shape["grp"], 16, 2, mesh.shape["tp"]),
        ("grp", "sp_0", "sp_1", "tp"),
    )
    return jax.shard_map(
        local,
        mesh=finer,
        in_specs=(
            P(GRP_SP, "tp"),
            P(GRP_SP, "tp"),
            P(GRP_SP, "tp"),
            P(GRP_SP, "tp"),
            P(GRP_SP, "tp"),
            P(GRP_SP, "tp"),
            P(GRP_SP, "tp"),
            P("tp"),
            P("tp"),
            P("tp"),
            P("tp"),
            P("tp", None),
            P(GRP_SP_TP, None),
            P(),
            P(GRP_SP_TP, None),
            P(GRP_SP_TP, None),
            P(SP, None, "tp"),
            P(SP, None, "tp"),
            P(SP, "tp", None),
        ),
        out_specs=P(GRP_SP_TP, None),
        check_vma=False,
    )
```

profile of v0, /device:TPU:33, one launch (start us, length us, event | category | flops | bytes accessed | tf_op | source)
XLA Modules:
  0.0 826.4 jit_solution(6993263350286761143)
XLA Ops:
  18.9 3.9 fusion.18
  25.6 5.9 fusion.15
  31.6 5.4 fusion.161
  46.3 4.4 add_add_fusion.1
  50.8 4.5 fusion.168
  62.4 3.8 fusion.171
  66.1 3.6 fusion.170
  73.1 5.5 convolution_add_fusion
  82.8 5.0 fusion.173
  91.1 5.2 multiply_add_fusion
  96.3 6.4 bitcast_add_fusion.2
  102.8 54.3 %while.17 = (s32[]{:T(128)}, f32[8,64,64]{1,2,0:T(8,128)S(1)}, f32[8,64,64]{1,2,0:T(8,128)}, f32[8,8,64,64]{2,3,1,0:T(8,128)}, f32[8,8,64,64]{2,3,1,0:T(8,128)},...) while((s32[]{:T(128)}, f32[8,64,64]{1,2,0:T(8,128)S(1)}, ...), condition=%wide.region_3.4_spmd.clone, body=%wide.region_2.3_spmd.clone.sunk | while | flops 50429952 | bytes 3016300 | solution.py:184
  157.2 22.3 %all-gather = f32[16,64,64]{2,1,0:T(8,128)S(1)} all-gather(f32[8,64,64]{2,1,0:T(8,128)S(1)} %copy.265), channel_id=2, replica_groups=mesh['grp'=2,'sp_0'=16,'sp_1'=2,'tp'=4] {'sp_1'}, dimensions={0}, use_global_device_ids=true | all-gather | bytes 393216 | tf_op jit(solution)/shard_map/all_gather | solution.py:29
  192.2 7.0 fusion.160
  199.2 4.9 fusion.40
  204.1 3.7 fusion.42
  207.8 6.2 fusion.159
  213.9 29.6 %all-gather.13.cloned.1.call-done = f32[128,64,64]{2,1,0:T(8,128)} async-done(((f32[8,64,64]{2,1,0:T(8,128)}), f32[128,64,64]{2,1,0:T(8,128)}) %all-gather.13.cloned.1.call-update) | async-done | bytes 2097168 | tf_op jit(solution)/shard_map/all_gather | solution.py:29
  243.5 75.4 %all-gather.15.cloned.1.call-done = f32[128,64,64]{2,1,0:T(8,128)} async-done(((f32[8,64,64]{2,1,0:T(8,128)}), f32[128,64,64]{2,1,0:T(8,128)}) %all-gather.15.cloned.1.call-update) | async-done | bytes 2097168 | tf_op jit(solution)/shard_map/all_gather | solution.py:29
  344.5 4.7 fusion.14
  359.4 4.3 fusion.96
  363.7 5.1 all-to-all-start
  370.6 37.4 %all-to-all-done = f32[4,128,2048]{2,1,0:T(8,128)} async-done(((f32[4,128,2048]{2,1,0:T(8,128)}), f32[4,128,2048]{2,1,0:T(8,128)}, u32[]{:S(2)}, u32[]{:S(2)}) %all-to-all-start) | async-done | bytes 4194336 | tf_op jit(solution)/shard_map/all_to_all | solution.py:46
  419.6 72.9 %all_to_all.35 = bf16[32,6,2048]{2,1,0:T(8,128)(2,1)S(1)} all-to-all(bf16[32,6,2048]{2,1,0:T(8,128)(2,1)S(1)} %get-tuple-element.144), channel_id=1, replica_groups=mesh['grp'=2,'sp_0'=16,'sp_1'=2,'tp'=4] {'sp_0','sp_1'}, dimensions={0} | all-to-all | bytes 1572864 | tf_op jit(solution)/shard_map/all_to_all | solution.py:69
  494.0 59.9 %all_to_all.36 = bf16[32,6,2048]{2,1,0:T(8,128)(2,1)S(1)} all-to-all(bf16[32,6,2048]{2,1,0:T(8,128)(2,1)} %get-tuple-element.145), channel_id=1, replica_groups=mesh['grp'=2,'sp_0'=16,'sp_1'=2,'tp'=4] {'sp_0','sp_1'}, dimensions={0} | all-to-all | bytes 1572864 | tf_op jit(solution)/shard_map/all_to_all | solution.py:69
  555.4 5.6 copy.278
  561.0 6.4 reshape.180
  567.4 4.1 fusion.68
  571.5 7.9 convolution_convert_fusion.1
  579.4 6.3 reshape.181
  585.7 5.7 copy.279
  591.4 5.0 all-to-all-start.2
  596.4 5.6 copy.282
  602.0 6.3 reshape.183
  608.3 4.1 fusion.66
  612.4 7.7 convolution_convert_fusion
  620.1 6.2 reshape.184
  626.3 5.7 copy.283
  632.9 4.7 all-to-all-start.5
  643.8 29.5 %all-to-all-done.5 = bf16[4,32,6,2048]{3,1,2,0:T(8,128)(2,1)} async-done(((bf16[4,32,6,2048]{3,1,2,0:T(8,128)(2,1)}), bf16[4,32,6,2048]{3,1,2,0:T(8,128)(2,1)}, u32[]{:S(2)}, u32[]{:S(2)}) %all-to-all-start.5) | async-done | bytes 3145760 | tf_op jit(solution)/shard_map/all_to_all | solution.py:52
  673.3 8.6 %all-to-all-start.3 = ((bf16[32,6,2048]{2,1,0:T(8,128)(2,1)}), bf16[32,6,2048]{2,1,0:T(8,128)(2,1)}, u32[]{:S(2)}, u32[]{:S(2)}) async-start(bf16[32,6,2048]{2,1,0:T(8,128)(2,1)} %copy.280), calls=%async_computation.3 | async-start | bytes 2097152 | tf_op jit(solution)/shard_map/all_to_all | solution.py:280
  688.1 49.4 %all-to-all-done.3 = bf16[32,6,2048]{2,1,0:T(8,128)(2,1)} async-done(((bf16[32,6,2048]{2,1,0:T(8,128)(2,1)}), bf16[32,6,2048]{2,1,0:T(8,128)(2,1)}, u32[]{:S(2)}, u32[]{:S(2)}) %all-to-all-start.3) | async-done | bytes 786464 | tf_op jit(solution)/shard_map/all_to_all | solution.py:280
  737.5 5.1 all-to-all-start.6
  743.2 55.0 %all-to-all-done.6 = bf16[32,6,2048]{2,1,0:T(8,128)(2,1)} async-done(((bf16[32,6,2048]{2,1,0:T(8,128)(2,1)}), bf16[32,6,2048]{2,1,0:T(8,128)(2,1)}, u32[]{:S(2)}, u32[]{:S(2)}) %all-to-all-start.6) | async-done | bytes 786464 | tf_op jit(solution)/shard_map/all_to_all | solution.py:280
  798.2 3.7 pad_maximum_fusion
  801.9 3.6 reshape.186
  805.5 4.9 gather_fusion
  813.0 5.5 multiply_reduce_fusion
  (260 shorter events, 177.7 us)
Async XLA Ops:
  6.5 352.8 %copy-start = (bf16[512,2048]{1,0:T(8,128)(2,1)S(1)}, bf16[512,2048]{1,0:T(8,128)(2,1)}, u32[]{:S(2)}) copy-start(bf16[512,2048]{1,0:T(8,128)(2,1)} %param.32) | copy-start | bytes 6291460
  6.6 237.0 %all-gather.13.cloned.1.call-start = ((), (), s32[]{:S(2)}) async-start(), calls=%async_computation.9 | async-start | bytes 4456448 | tf_op jit(solution)/shard_map/all_gather | solution.py:29
  6.6 3.8 copy-start.39
  12.6 2.6 copy-start.35
  15.2 3.5 copy-start.43
  18.8 3.9 copy-start.38
  18.8 3.9 copy-start.42
  25.6 6.0 copy-start.1
  25.6 6.0 copy-start.5
  31.5 5.4 copy-start.10
  31.5 5.4 copy-start.13
  50.7 4.6 copy-start.12
  50.8 4.6 copy-start.18
  62.4 3.8 copy-start.19
  66.1 3.7 copy-start.37
  73.1 14.8 %copy-start.20 = (bf16[8,8,64,64]{2,3,1,0:T(8,128)(2,1)}, bf16[8,8,64,64]{2,3,1,0:T(8,128)(2,1)S(1)}, u32[]{:S(2)}) copy-start(bf16[8,8,64,64]{2,3,1,0:T(8,128)(2,1)S(1)} %copy.269) | copy-start | bytes 1572868
  73.1 5.5 copy-start.14
  81.0 10.1 %copy-start.15 = (f32[8,8,64,64]{3,2,1,0:T(8,128)}, f32[8,8,64,64]{3,2,1,0:T(8,128)S(1)}, u32[]{:S(2)}) copy-start(f32[8,8,64,64]{3,2,1,0:T(8,128)S(1)} %fusion.172) | copy-start | bytes 3145732
  82.8 5.1 copy-start.2
  82.8 5.1 copy-start.6
  87.9 3.2 copy-start.11
  181.0 8.0 copy-start.22
  182.2 136.7 %all-gather.15.cloned.1.call-start = ((), (), s32[]{:S(2)}) async-start(), calls=%async_computation.10 | async-start | bytes 4456448 | tf_op jit(solution)/shard_map/all_gather | solution.py:29
  185.6 5.1 copy-start.44
  192.2 7.0 copy-start.17
  199.2 4.9 copy-start.16
  204.0 3.7 copy-start.3
  204.0 3.7 copy-start.7
  204.0 3.7 copy-start.8
  318.9 7.2 copy-start.29
  339.6 2.5 copy-start.33
  339.6 4.5 copy-start.34
  341.3 2.8 copy-start.26
  342.1 2.4 copy-start.9
  344.5 4.7 copy-start.21
  344.5 4.7 copy-start.23
  344.5 4.7 copy-start.25
  363.7 5.1 copy-start.40
  363.7 44.3 %all-to-all-start = ((f32[4,128,2048]{2,1,0:T(8,128)}), f32[4,128,2048]{2,1,0:T(8,128)}, u32[]{:S(2)}, u32[]{:S(2)}) async-start(f32[4,128,2048]{2,1,0:T(8,128)} %bitcast.197), calls=%async_computation | async-start | bytes 8388608 | tf_op jit(solution)/shard_map/all_to_all | solution.py:46
  368.8 186.6 %all-gather.9.cloned.1.call-start = ((), (), s32[]{:S(2)}) async-start(), calls=%async_computation.7 | async-start | bytes 3932160 | tf_op jit(solution)/shard_map/all_gather | solution.py:277
  370.5 40.1 %copy-start.28 = (bf16[128,2048]{1,0:T(8,128)(2,1)S(1)}, bf16[128,2048]{1,0:T(8,128)(2,1)}, u32[]{:S(2)}) copy-start(bf16[128,2048]{1,0:T(8,128)(2,1)} %param.33) | copy-start | bytes 1572868
  370.5 40.4 %copy-start.41 = (f32[2048]{0:T(1024)S(1)}, f32[2048]{0:T(1024)}, u32[]{:S(2)}) copy-start(f32[2048]{0:T(1024)} %param.34) | copy-start | bytes 24580
  494.0 102.4 %all-gather.11.cloned.1.call-start = ((), (), s32[]{:S(2)}) async-start(), calls=%async_computation.8 | async-start | bytes 3932160 | tf_op jit(solution)/shard_map/all_gather | solution.py:277
  591.4 41.5 %all-to-all-start.2 = ((bf16[4,32,6,2048]{3,1,2,0:T(8,128)(2,1)}), bf16[4,32,6,2048]{3,1,2,0:T(8,128)(2,1)}, u32[]{:S(2)}, u32[]{:S(2)}) async-start(bf16[4,32,6,2048]{3,1,2,0:T(8,128)(2,1)} %copy.279), calls=%async_computation.2 | async-start | bytes 6291456 | tf_op jit(solution)/shard_map/all_to_all | solution.py:52
  632.9 40.4 %all-to-all-start.5 = ((bf16[4,32,6,2048]{3,1,2,0:T(8,128)(2,1)}), bf16[4,32,6,2048]{3,1,2,0:T(8,128)(2,1)}, u32[]{:S(2)}, u32[]{:S(2)}) async-start(bf16[4,32,6,2048]{3,1,2,0:T(8,128)(2,1)} %copy.283), calls=%async_computation.5 | async-start | bytes 6291456 | tf_op jit(solution)/shard_map/all_to_all | solution.py:52
  673.3 64.2 %all-to-all-start.3 = ((bf16[32,6,2048]{2,1,0:T(8,128)(2,1)}), bf16[32,6,2048]{2,1,0:T(8,128)(2,1)}, u32[]{:S(2)}, u32[]{:S(2)}) async-start(bf16[32,6,2048]{2,1,0:T(8,128)(2,1)} %copy.280), calls=%async_computation.3 | async-start | bytes 2097152 | tf_op jit(solution)/shard_map/all_to_all | solution.py:280
  685.6 57.5 %copy-start.45 = (f32[128,2]{0,1:T(2,128)S(1)}, f32[128,2]{0,1:T(2,128)}, u32[]{:S(2)}) copy-start(f32[128,2]{0,1:T(2,128)} %param.36) | copy-start | bytes 3076
  737.5 60.7 %all-to-all-start.6 = ((bf16[32,6,2048]{2,1,0:T(8,128)(2,1)}), bf16[32,6,2048]{2,1,0:T(8,128)(2,1)}, u32[]{:S(2)}, u32[]{:S(2)}) async-start(bf16[32,6,2048]{2,1,0:T(8,128)(2,1)} %copy.284), calls=%async_computation.6 | async-start | bytes 2097152 | tf_op jit(solution)/shard_map/all_to_all | solution.py:280
  (7 other events, 11.0 us)
Sparse Core Ops, SparseCore 0:
  182.3 61.1 all-gather.12
  245.3 73.5 all-gather.14
  494.1 35.1 all-gather.8
  555.5 35.0 all-gather.10
where the time goes:
time: 836 us; the launch traced here: 826 us
  waiting for transfers between devices  277 us (33%)
  matrix products  188 us (22%)
  blocking collectives  157 us (19%)
  local copies, waits for them, and re-layouts  113 us (14%)
  other arithmetic  47.5 us (6%)
  starting transfers between devices  28.7 us (3%)
  between operations  14.6 us (2%)
    all_to_all x2, blocking collectives, exchange_in_groups(): lax.all_to_all(group, axis, split_axis=split_dim, concat_axis=concat_dim,...  133 us
    all_gather x2, waiting for transfers between devices, prefix_by_axis(): pieces = jax.tree.map(lambda part: lax.all_gather(part, axis), so_far)  105 us
    all_to_all x2, waiting for transfers between devices, serve_group(): lax.all_to_all(summed.astype(jnp.bfloat16), SP, split_axis=0, concat_axis...  104 us
    dot_general x28, matrix products, chain_combine(): jnp.einsum('hij,hjk->hik', earlier[1], later[0], precision=PRECISE)  44.6 us
    all_to_all x1, waiting for transfers between devices, summed_on_arrival(): lax.all_to_all(parts, axis, split_axis=0, concat_axis=0, tiled=True)  37.4 us
    dot_general x10, matrix products, square_blocks(): return jnp.einsum('bhts,bhsu->bhtu', left, right, precision=PRECISE)  34.7 us
    all_to_all x2, waiting for transfers between devices, sent_and_summed(): lax.all_to_all(parts, axis, split_axis=0, concat_axis=0, tiled=True)  30.4 us
    all_gather x2, blocking collectives, prefix_by_axis(): pieces = jax.tree.map(lambda part: lax.all_gather(part, axis), so_far)  24.5 us
  transfers between devices with their start and end apart: 9, of which 7 were waited for; matrix products, arithmetic and copies ran while one was open for 14% of the time, Pallas kernels for 0%

commit v1 on v0

v1 whole, which is shorter than its diff:
```python
import functools

import jax
import jax.numpy as jnp
from jax import lax
from jax.experimental import pallas as pl
from jax.experimental.pallas import tpu as pltpu
from jax.sharding import PartitionSpec as P

f32, bf16 = jnp.float32, jnp.bfloat16
MESH = pl.DeviceIdType.MESH
NN = (((1,), (0,)), ((), ()))
NT = (((1,), (1,)), ((), ()))
GROUP_EPS = 0.00064
NORM_EPS = 1e-06
SPAN = 64
LANES = 128
HEAD = 64
DECAY_SCALE = 0.6065306597126334
QUARTERS = 4
BLOCK = 4
VMEM_SPEC = pl.BlockSpec(memory_space=pltpu.VMEM)


def dot(a, b, dims=NN):
    return lax.dot_general(a.astype(bf16), b.astype(bf16), dims, preferred_element_type=f32)


def halves(x):
    high = x.astype(bf16)
    return high, (x - high.astype(f32)).astype(bf16)


def dot_split_left(a, b):
    high, low = halves(a)
    return dot(high, b) + dot(low, b)


def dot_split_right(a, b):
    high, low = halves(b)
    return dot(a, high) + dot(a, low)


def iota(shape, dim):
    return lax.broadcasted_iota(jnp.int32, shape, dim)


def sigmoid(x):
    return 1.0 / (1.0 + jnp.exp(-x))


def head_ones():
    shape = (LANES, LANES)
    return jnp.where((iota(shape, 0) >> 6) == (iota(shape, 1) >> 6), 1.0, 0.0).astype(bf16)


def stacked(x):
    first = iota(x.shape, 1) < HEAD
    zero = jnp.zeros_like(x)
    return jnp.concatenate([jnp.where(first, x, zero), jnp.where(first, zero, x)], axis=0)


def chunk_maps(recept, key, value, decay_pre, rate_pre, offset, decay_bias, rate_bias):
    row = iota((SPAN, LANES), 0)
    col = iota((SPAN, LANES), 1) & (HEAD - 1)
    decay_log = offset - DECAY_SCALE * sigmoid(decay_bias + decay_pre)
    rate = sigmoid(rate_bias + rate_pre)
    norm = dot_split_left(key * key, head_ones())
    unit = key * lax.rsqrt(norm + NORM_EPS)
    square = (SPAN, SPAN)
    lower = jnp.where(iota(square, 0) >= iota(square, 1), 1.0, 0.0).astype(bf16)
    cumul = dot_split_right(lower, decay_log)
    middle = cumul[SPAN // 2 - 1 : SPAN // 2, :]
    rel = cumul - middle
    rise, fall = jnp.exp(rel), jnp.exp(-rel)
    to_middle = jnp.exp(middle)
    to_end = jnp.exp(cumul[SPAN - 1 : SPAN, :] - middle)
    remove = -unit * jnp.exp(rel - decay_log)
    read = recept * rise
    write = unit * rate * fall
    keys = key * fall
    scores = dot(
        jnp.concatenate([remove.astype(bf16), read.astype(bf16)], axis=0),
        jnp.concatenate([stacked(write.astype(bf16)), stacked(keys.astype(bf16))], axis=0),
        NT,
    )
    strict, within = row > col, row >= col
    lower_part = jnp.where(strict, scores[:SPAN, :LANES], 0.0)
    remove_key = jnp.where(strict, scores[:SPAN, LANES:], 0.0)
    read_write = jnp.where(within, scores[SPAN:, :LANES], 0.0)
    read_key = jnp.where(within, scores[SPAN:, LANES:], 0.0)

    def merging(level):
        size = 1 << level
        same = (row >> (level + 1)) == (col >> (level + 1))
        return same & ((row & size) != 0) & ((col & size) == 0)

    inverse = jnp.where(row == col, 1.0, jnp.where(merging(0), lower_part, 0.0))
    for level in range(1, SPAN.bit_length() - 1):
        block = jnp.where(merging(level), lower_part, 0.0)
        inner = dot(block, stacked(inverse.astype(bf16)))
        inverse = inverse + dot(inverse, stacked(inner.astype(bf16)))
    removed_value = dot(remove_key, stacked(value.astype(bf16)))
    solved = dot(
        inverse,
        jnp.concatenate(
            [stacked((remove * to_middle).astype(bf16)), stacked(removed_value.astype(bf16))], axis=1
        ),
    )
    left = jnp.concatenate([solved[:, :LANES], read * to_middle], axis=0).astype(bf16)
    write_end = jnp.concatenate([write * to_end, keys * to_end], axis=0).T.astype(bf16)
    ending = jnp.broadcast_to(to_end * to_middle, (LANES, LANES)).T
    within_maps = jnp.concatenate([read_write, read_key], axis=1).astype(bf16)
    return left, solved[:, LANES:], within_maps, write_end, ending


def mixer_kernel(
    pairs, chunks,
    recept_ref, key_ref, value_ref, decay_ref, rate_ref, offset_ref, decay_bias_ref, rate_bias_ref,
    summary_ref, map_ref, own_ref,
    left_ref, solved_ref, within_ref, write_ref, ending_ref, state_ref, removed_ref, partial_ref,
):
    first_head = iota((SPAN, LANES), 1) < HEAD

    def rows_of(c):
        return pl.ds(pl.multiple_of(c * SPAN, SPAN), SPAN)

    def prepare(c):
        rows = rows_of(c)
        for p in range(pairs):
            cols = slice(p * LANES, (p + 1) * LANES)
            offset = jnp.where(
                first_head, offset_ref[rows, 2 * p : 2 * p + 1], offset_ref[rows, 2 * p + 1 : 2 * p + 2]
            )
            left, solved, within, write, ending = chunk_maps(
                recept_ref[rows, cols].astype(f32),
                key_ref[rows, cols].astype(f32),
                value_ref[rows, cols].astype(f32),
                decay_ref[rows, cols].astype(f32),
                rate_ref[rows, cols].astype(f32),
                offset,
                decay_bias_ref[:, cols],
                rate_bias_ref[:, cols],
            )
            left_ref[c, p] = left
            solved_ref[c, p] = solved
            within_ref[c, p] = within
            write_ref[c, p] = write
            ending_ref[c, p] = ending

    unroll = 2 if chunks % 2 == 0 else 1

    def prepare_some(i, _):
        for k in range(unroll):
            prepare(i * unroll + k)
        return 0

    lax.fori_loop(0, chunks // unroll, prepare_some, 0)

    square = (LANES, LANES)
    eye = jnp.where(iota(square, 0) == iota(square, 1), 1.0, 0.0)
    for p in range(pairs):
        state_ref[p, :, :LANES] = eye
        state_ref[p, :, LANES:] = jnp.zeros(square, f32)
    own_block = (iota((LANES, 2 * LANES), 0) >> 6) == ((iota((LANES, 2 * LANES), 1) >> 6) & 1)

    def advance(c, _):
        rows = rows_of(c)
        for p in range(pairs):
            value = value_ref[rows, p * LANES : (p + 1) * LANES]
            state = state_ref[p]
            crossed = dot(left_ref[c, p], state)
            removed = jnp.concatenate(
                [crossed[:SPAN, :LANES], crossed[:SPAN, LANES:] + solved_ref[c, p]], axis=1
            ).astype(bf16)
            removed_ref[c, p] = removed
            partial_ref[c, p] = crossed[SPAN:]
            right = jnp.concatenate(
                [removed, jnp.concatenate([jnp.zeros_like(value), value], axis=1)], axis=0
            )
            update = dot(write_ref[c, p], right)
            ending = ending_ref[c, p]
            state_ref[p] = state * jnp.concatenate([ending, ending], axis=1) + jnp.where(
                own_block, update, 0.0
            )
        return 0

    lax.fori_loop(0, chunks, advance, 0)

    for p in range(pairs):
        transit = state_ref[p, :, :LANES] - eye
        added = state_ref[p, :, LANES:]
        summary_ref[p, 0] = (transit[:HEAD] + transit[HEAD:]).astype(bf16)
        summary_ref[p, 1] = (added[:HEAD] + added[HEAD:]).astype(bf16)

    def emit(c, _):
        rows = rows_of(c)
        for p in range(pairs):
            cols = slice(p * LANES, (p + 1) * LANES)
            removed = removed_ref[c, p]
            value = stacked(value_ref[rows, cols])
            right = jnp.concatenate(
                [
                    jnp.concatenate([stacked(removed[:, :LANES]), stacked(removed[:, LANES:])], axis=1),
                    jnp.concatenate([jnp.zeros_like(value), value], axis=1),
                ],
                axis=0,
            )
            both = partial_ref[c, p] + dot(within_ref[c, p], right)
            map_ref[rows, cols] = both[:, :LANES].astype(bf16)
            own_ref[rows, cols] = both[:, LANES:]
        return 0

    lax.fori_loop(0, chunks, emit, 0)


def mixer_local(recept, key, value, decay, rate, offset, decay_bias, rate_bias):
    length, width = recept.shape
    pairs, chunks = width // LANES, length // SPAN
    per = (chunks, pairs)
    return pl.pallas_call(
        functools.partial(mixer_kernel, pairs, chunks),
        name="mixer_local",
        out_shape=(
            jax.ShapeDtypeStruct((pairs, 2, HEAD, LANES), bf16),
            jax.ShapeDtypeStruct((length, width), bf16),
            jax.ShapeDtypeStruct((length, width), f32),
        ),
        in_specs=[VMEM_SPEC] * 8,
        out_specs=(VMEM_SPEC,) * 3,
        scratch_shapes=[
            pltpu.VMEM(per + (2 * SPAN, LANES), bf16),
            pltpu.VMEM(per + (SPAN, LANES), f32),
            pltpu.VMEM(per + (SPAN, 2 * LANES), bf16),
            pltpu.VMEM(per + (LANES, 2 * SPAN), bf16),
            pltpu.VMEM(per + (LANES, LANES), f32),
            pltpu.VMEM((pairs, LANES, 2 * LANES), f32),
            pltpu.VMEM(per + (SPAN, 2 * LANES), bf16),
            pltpu.VMEM(per + (SPAN, 2 * LANES), f32),
        ],
        compiler_params=pltpu.CompilerParams(vmem_limit_bytes=40 << 20),
        cost_estimate=pl.CostEstimate(
            flops=80 * 2 * LANES * length * width, bytes_accessed=12 * length * width, transcendentals=0
        ),
    )(recept, key, value, decay, rate, offset, decay_bias, rate_bias)


def prefix_kernel(n, pairs, summary_ref, enter_ref, got, states, entry, sent1, came1, sent2, came2):
    me = lax.axis_index("sp")
    stride = n // pairs
    works = lax.rem(me, stride) == 0
    mine = lax.div(me, stride)
    barrier = pltpu.get_barrier_semaphore()

    def greet(device):
        pl.semaphore_signal(barrier, inc=1, device_id={"sp": device}, device_id_type=MESH)

    @pl.when(works)
    def _():
        def body(j, _):
            greet(lax.rem(me + j, n))
            return 0

        lax.fori_loop(1, n, body, 0)
        pl.semaphore_wait(barrier, n - 1)

    @pl.when(jnp.logical_not(works))
    def _():
        for p in range(pairs):
            greet(p * stride)
        pl.semaphore_wait(barrier, pairs)

    def outward(p):
        return pltpu.make_async_remote_copy(
            src_ref=summary_ref.at[p], dst_ref=got.at[me], send_sem=sent1.at[p], recv_sem=came1.at[me],
            device_id={"sp": p * stride}, device_id_type=MESH,
        )

    def inward(i):
        return pltpu.make_async_remote_copy(
            src_ref=summary_ref.at[0], dst_ref=got.at[i], send_sem=sent1.at[0], recv_sem=came1.at[i],
            device_id={"sp": i}, device_id_type=MESH,
        )

    def back(i, p):
        return pltpu.make_async_remote_copy(
            src_ref=states.at[i], dst_ref=entry.at[p], send_sem=sent2.at[i], recv_sem=came2.at[p],
            device_id={"sp": i}, device_id_type=MESH,
        )

    for p in range(pairs):
        @pl.when(me != p * stride)
        def _():
            outward(p).start()

        @pl.when(me == p * stride)
        def _():
            got[me] = summary_ref[p]

    @pl.when(works)
    def _():
        def step(i, state):
            states[i] = state.astype(bf16)

            @pl.when(i != me)
            def _():
                back(i, mine).start()
                inward(i).wait_recv()

            @pl.when(i == me)
            def _():
                entry[mine] = states[i]

            high, low = halves(state)
            transit, added = got[i, 0], got[i, 1].astype(f32)
            moved = dot(transit, stacked(high)) + dot(transit, stacked(low))
            return state + (moved + added)

        lax.fori_loop(0, n, step, jnp.zeros((HEAD, LANES), f32))

    for p in range(pairs):
        @pl.when(me != p * stride)
        def _():
            back(0, p).wait_recv()

        enter_ref[p] = entry[p]

    for p in range(pairs):
        @pl.when(me != p * stride)
        def _():
            outward(p).wait_send()

    @pl.when(works)
    def _():
        def body(i, _):
            @pl.when(i != me)
            def _():
                back(i, mine).wait_send()

            return 0

        lax.fori_loop(0, n, body, 0)


def prefix_states(summary, n):
    pairs = summary.shape[0]
    return pl.pallas_call(
        functools.partial(prefix_kernel, n, pairs),
        name="prefix_states",
        out_shape=jax.ShapeDtypeStruct((pairs, HEAD, LANES), bf16),
        in_specs=[VMEM_SPEC],
        out_specs=VMEM_SPEC,
        scratch_shapes=[
            pltpu.VMEM((n, 2, HEAD, LANES), bf16),
            pltpu.VMEM((n, HEAD, LANES), bf16),
            pltpu.VMEM((pairs, HEAD, LANES), bf16),
            pltpu.SemaphoreType.DMA((pairs,)),
            pltpu.SemaphoreType.DMA((n,)),
            pltpu.SemaphoreType.DMA((n,)),
            pltpu.SemaphoreType.DMA((pairs,)),
        ],
        compiler_params=pltpu.CompilerParams(collective_id=0, has_side_effects=True),
        cost_estimate=pl.CostEstimate(flops=10**9, bytes_accessed=60 << 20, transcendentals=0),
    )(summary)


def readout_kernel(
    pairs, length, recept_ref, key_ref, value_ref, gate_ref, gain_ref, self_ref, map_ref, own_ref,
    enter_ref, out_ref,
):
    ones = head_ones()
    for p in range(pairs):
        cols = slice(p * LANES, (p + 1) * LANES)
        state = stacked(enter_ref[p])
        for start in range(0, length, 128):
            rows = slice(start, start + 128)
            value = value_ref[rows, cols].astype(f32)
            own = recept_ref[rows, cols].astype(f32) * key_ref[rows, cols].astype(f32) * self_ref[:, cols]
            own = dot_split_left(own, ones) * value
            read = dot(map_ref[rows, cols], state) + own_ref[rows, cols]
            center = read - dot_split_left(read, ones) * (1.0 / HEAD)
            spread = dot_split_left(center * center, ones) * (1.0 / HEAD)
            normed = center * lax.rsqrt(spread + GROUP_EPS) * gain_ref[:, cols]
            out_ref[rows, cols] = ((normed + own) * gate_ref[rows, cols].astype(f32)).astype(bf16)


def readout(recept, key, value, gate, gain, self_weight, maps, own, enter):
    length, width = recept.shape
    return pl.pallas_call(
        functools.partial(readout_kernel, width // LANES, length),
        name="readout",
        out_shape=jax.ShapeDtypeStruct((length, width), bf16),
        in_specs=[VMEM_SPEC] * 9,
        out_specs=VMEM_SPEC,
        cost_estimate=pl.CostEstimate(flops=10**9, bytes_accessed=16 << 20, transcendentals=0),
    )(recept, key, value, gate, gain, self_weight, maps, own, enter)


def route_columns(index_ref, experts, capacity):
    rows = index_ref.shape[0]
    lane = iota((rows, LANES), 1)
    first = lane == index_ref[:, 0:1]
    second = lane == index_ref[:, 1:2]
    square = (rows, rows)
    before = jnp.where(iota(square, 0) > iota(square, 1), 1.0, 0.0)
    both = jnp.where(first, 1.0, 0.0) + jnp.where(second, 1.0, 0.0)
    counts = dot(before, both) + (lane * capacity).astype(f32)
    return [jnp.sum(jnp.where(hit, counts, 0.0), axis=1, keepdims=True) for hit in (first, second)]


def build_kernel(experts, capacity, residual_ref, proj_ref, gain_ref, index_ref, out_ref, stack_ref):
    rows, width = residual_ref.shape
    part = width // QUARTERS
    stream = residual_ref[...].astype(f32) + proj_ref[...].astype(f32)
    scale = lax.rsqrt(jnp.mean(stream * stream, axis=1, keepdims=True) + NORM_EPS)
    ffn_in = (stream * scale * gain_ref[...]).astype(bf16)
    for q in range(QUARTERS):
        stack_ref[q * rows : (q + 1) * rows] = ffn_in[:, q * part : (q + 1) * part]
    targets = [
        jnp.broadcast_to(t, (rows, rows)).T[:1] for t in route_columns(index_ref, experts, capacity)
    ]
    block = QUARTERS * capacity
    many = BLOCK * block
    line = iota((many, 1), 0)
    device = lax.div(line, block)
    quarter = lax.div(lax.rem(line, block), capacity)
    slot = (device * capacity + lax.rem(line, capacity)).astype(f32)
    for g in range(experts // BLOCK):
        wanted = slot + float(g * BLOCK * capacity)
        hit = jnp.where((wanted == targets[0]) | (wanted == targets[1]), 1.0, 0.0)
        place = jnp.concatenate(
            [jnp.where(quarter == q, hit, 0.0) for q in range(QUARTERS)], axis=1
        ).astype(bf16)
        lines = dot(place, stack_ref[...]).astype(bf16)
        for k in range(BLOCK):
            out_ref[g * BLOCK + k] = lines[k * block : (k + 1) * block]


def build(residual, proj, gain, index, experts, capacity):
    rows, width = residual.shape
    return pl.pallas_call(
        functools.partial(build_kernel, experts, capacity),
        name="build",
        out_shape=jax.ShapeDtypeStruct((experts, QUARTERS * capacity, width // QUARTERS), bf16),
        in_specs=[VMEM_SPEC] * 4,
        out_specs=VMEM_SPEC,
        scratch_shapes=[pltpu.VMEM((QUARTERS * rows, width // QUARTERS), bf16)],
        cost_estimate=pl.CostEstimate(flops=10**9, bytes_accessed=8 << 20, transcendentals=0),
    )(residual, proj, gain, index)


def exchange_kernel(n, src_ref, out_ref, own_sem, sent, came):
    me = lax.axis_index("sp")
    barrier = pltpu.get_barrier_semaphore()

    def greet(k, _):
        pl.semaphore_signal(
            barrier, inc=1, device_id={"sp": lax.rem(me + k, n)}, device_id_type=MESH
        )
        return 0

    lax.fori_loop(1, n, greet, 0)
    own = pltpu.make_async_copy(src_ref.at[me], out_ref.at[me], own_sem)
    own.start()
    pl.semaphore_wait(barrier, n - 1)

    def copy(k):
        to = lax.rem(me + k, n)
        return pltpu.make_async_remote_copy(
            src_ref=src_ref.at[to], dst_ref=out_ref.at[me], send_sem=sent.at[k], recv_sem=came.at[k],
            device_id={"sp": to}, device_id_type=MESH,
        )

    def start(k, _):
        away = n // 2 - lax.div(k, 2)
        copy(jnp.where(lax.rem(k, 2) == 0, away, n - away)).start()
        return 0

    def arrived(k):
        frm = lax.rem(me + n - k, n)
        return pltpu.make_async_remote_copy(
            src_ref=src_ref.at[frm], dst_ref=out_ref.at[frm], send_sem=sent.at[k], recv_sem=came.at[k],
            device_id={"sp": frm}, device_id_type=MESH,
        )

    copy(n // 2).start()
    lax.fori_loop(2, n, start, 0)
    own.wait()

    def finish(k, _):
        arrived(k).wait_recv()
        copy(k).wait_send()
        return 0

    lax.fori_loop(1, n, finish, 0)


def exchange(blocks, n, number):
    return pl.pallas_call(
        functools.partial(exchange_kernel, n),
        name=f"exchange_{number}",
        out_shape=jax.ShapeDtypeStruct(blocks.shape, blocks.dtype),
        in_specs=[VMEM_SPEC],
        out_specs=VMEM_SPEC,
        scratch_shapes=[
            pltpu.SemaphoreType.DMA,
            pltpu.SemaphoreType.DMA((n,)),
            pltpu.SemaphoreType.DMA((n,)),
        ],
        compiler_params=pltpu.CompilerParams(collective_id=number, has_side_effects=True),
        cost_estimate=pl.CostEstimate(flops=10**6, bytes_accessed=200 << 20, transcendentals=0),
    )(blocks)


def reorder(capacity, to_rows):
    many = BLOCK * QUARTERS * capacity
    square = (many, many)
    out, line = (iota(square, 0), iota(square, 1)) if to_rows else (iota(square, 1), iota(square, 0))
    device, quarter = lax.div(line, QUARTERS * capacity), lax.rem(lax.div(line, capacity), QUARTERS)
    place = (quarter * BLOCK + device) * capacity + lax.rem(line, capacity)
    return jnp.where(out == place, 1.0, 0.0).astype(bf16)


def expert_kernel(n, capacity, came_ref, gate_ref, up_ref, down_ref, out_ref, rows_ref, total_ref):
    j = pl.program_id(0)
    block = QUARTERS * capacity
    height = BLOCK * capacity
    part = rows_ref.shape[1] // QUARTERS

    @pl.when(j == 0)
    def _():
        order = reorder(capacity, True)
        for g in range(n // BLOCK):
            lines = jnp.concatenate([came_ref[g * BLOCK + k] for k in range(BLOCK)], axis=0)
            moved = dot(order, lines).astype(bf16)
            for q in range(QUARTERS):
                rows_ref[g * height : (g + 1) * height, q * part : (q + 1) * part] = moved[
                    q * height : (q + 1) * height
                ]
        total_ref[...] = jnp.zeros_like(total_ref)

    gated = dot(rows_ref[...], gate_ref[0])
    upward = dot(rows_ref[...], up_ref[0])
    hidden = (gated * sigmoid(gated) * upward).astype(bf16)
    total_ref[...] += dot(hidden, down_ref[0])

    @pl.when(j == pl.num_programs(0) - 1)
    def _():
        order = reorder(capacity, False)
        for g in range(n // BLOCK):
            rows = slice(g * height, (g + 1) * height)
            lines = jnp.concatenate(
                [total_ref[rows, q * part : (q + 1) * part] for q in range(QUARTERS)], axis=0
            )
            moved = dot(order, lines).astype(bf16)
            for k in range(BLOCK):
                out_ref[g * BLOCK + k] = moved[k * block : (k + 1) * block]


def expert_rows(came, gate, up, down, capacity):
    n, block, part = came.shape
    pieces, width, units = gate.shape
    whole = pl.BlockSpec((n, block, part), lambda j: (0, 0, 0))
    return pl.pallas_call(
        functools.partial(expert_kernel, n, capacity),
        name="expert_rows",
        grid=(pieces,),
        out_shape=jax.ShapeDtypeStruct(came.shape, bf16),
        in_specs=[
            whole,
            pl.BlockSpec((1, width, units), lambda j: (j, 0, 0)),
            pl.BlockSpec((1, width, units), lambda j: (j, 0, 0)),
            pl.BlockSpec((1, units, width), lambda j: (j, 0, 0)),
        ],
        out_specs=whole,
        scratch_shapes=[
            pltpu.VMEM((n * capacity, width), bf16),
            pltpu.VMEM((n * capacity, width), f32),
        ],
        compiler_params=pltpu.CompilerParams(
            dimension_semantics=("arbitrary",), vmem_limit_bytes=40 << 20
        ),
        cost_estimate=pl.CostEstimate(flops=5 * 10**9, bytes_accessed=16 << 20, transcendentals=0),
    )(came, gate, up, down)


def combine_kernel(n, capacity, residual_ref, proj_ref, index_ref, weight_ref, back_ref, out_ref, rows_ref):
    rows, width = residual_ref.shape
    part = width // QUARTERS
    height = BLOCK * capacity
    order = reorder(capacity, True)
    for g in range(n // BLOCK):
        lines = jnp.concatenate([back_ref[g * BLOCK + k] for k in range(BLOCK)], axis=0)
        moved = dot(order, lines).astype(bf16)
        for q in range(QUARTERS):
            rows_ref[g * height : (g + 1) * height, q * part : (q + 1) * part] = moved[
                q * height : (q + 1) * height
            ]
    targets = route_columns(index_ref, n, capacity)
    slot = iota((rows, n * capacity), 1).astype(f32)
    mix = jnp.where(slot == targets[0], weight_ref[:, 0:1], 0.0) + jnp.where(
        slot == targets[1], weight_ref[:, 1:2], 0.0
    )
    high, low = halves(mix)
    for q in range(QUARTERS):
        cols = slice(q * part, (q + 1) * part)
        routed = dot(high, rows_ref[:, cols]) + dot(low, rows_ref[:, cols])
        stream = residual_ref[:, cols].astype(f32) + proj_ref[:, cols].astype(f32)
        out_ref[:, cols] = (stream + routed).astype(bf16)


def combine(residual, proj, index, weight, back, capacity):
    n = back.shape[0]
    return pl.pallas_call(
        functools.partial(combine_kernel, n, capacity),
        name="combine",
        out_shape=jax.ShapeDtypeStruct(residual.shape, bf16),
        in_specs=[VMEM_SPEC] * 5,
        out_specs=VMEM_SPEC,
        scratch_shapes=[pltpu.VMEM((n * capacity, residual.shape[1]), bf16)],
        cost_estimate=pl.CostEstimate(flops=10**9, bytes_accessed=8 << 20, transcendentals=0),
    )(residual, proj, index, weight, back)


def local(
    recept, key_input, value_input, output_gate_input, decay_input_part, correction_rate_input,
    head_decay_offset, decay_fixed_bias, correction_rate_bias, head_norm_gain, self_term_weight,
    output_weight_matrix, residual, feedforward_norm_gain, routed_expert_index, routed_expert_weight,
    gate_weight_experts, up_weight_experts, down_weight_experts,
):
    n = lax.axis_size("sp")
    out_weight = lax.all_gather(output_weight_matrix, "tp")
    gate = lax.all_gather(gate_weight_experts[0], "tp")
    up = lax.all_gather(up_weight_experts[0], "tp")
    down = lax.all_gather(down_weight_experts[0], "tp")

    summary, maps, own = mixer_local(
        recept, key_input, value_input, decay_input_part, correction_rate_input, head_decay_offset,
        decay_fixed_bias[None], correction_rate_bias[None],
    )
    enter = prefix_states(summary, n)
    mixed = readout(
        recept, key_input, value_input, output_gate_input, head_norm_gain[None], self_term_weight[None],
        maps, own, enter,
    )
    shares = mixed.reshape(lax.axis_size("tp"), -1, mixed.shape[1])
    shares = lax.all_to_all(shares, "tp", split_axis=0, concat_axis=0, tiled=True)
    proj = jnp.einsum("jrc,jcd->rd", shares, out_weight, preferred_element_type=f32).astype(bf16)

    rows = residual.shape[0]
    experts = gate_weight_experts.shape[0] * n
    capacity = 3 * rows // experts
    outgoing = build(residual, proj, feedforward_norm_gain[None], routed_expert_index, experts, capacity)
    came = exchange(outgoing, n, 1)
    results = expert_rows(came, gate, up, down, capacity)
    back = exchange(results, n, 2)
    return combine(residual, proj, routed_expert_index, routed_expert_weight, back, capacity)


def solution(mesh):
    shared = P(("grp", "sp", "tp"), None)
    split = P(("grp", "sp"), "tp")
    return jax.shard_map(
        local,
        mesh=mesh,
        in_specs=(split,) * 7 + (P("tp"),) * 4 + (P("tp", None), shared, P(), shared, shared)
        + (P("sp", None, "tp"), P("sp", None, "tp"), P("sp", "tp", None)),
        out_specs=shared,
        check_vma=False,
    )
```

time: 836 us -> 393 us (0.47); the launches traced: 826 us -> 393 us
  Pallas kernels: 0 us -> 298 us
  waiting for transfers between devices: 277 us -> 59.4 us
  matrix products: 188 us -> 6.14 us
  blocking collectives: 157 us -> 0 us
  local copies, waits for them, and re-layouts: 113 us -> 11 us
  other arithmetic: 47.5 us -> 0 us
  starting transfers between devices: 28.7 us -> 4.37 us
    pallas_call x0 -> x8, Pallas kernels: none -> 298 us  [the longest x2 174 us: exchange(): pl.pallas_call(functools.partial(exchange_kernel, n), name=f'exchange_{nu...]
    dot_general x70 -> x1, matrix products: 188 us -> 6.14 us  [local(): jnp.einsum('jrc,jcd->rd', shares, out_weight, preferred_element_type=f32)]
    all_to_all x5 -> x1, waiting for transfers between devices: 172 us -> 5.65 us  [local(): lax.all_to_all(shares, 'tp', split_axis=0, concat_axis=0, tiled=True)]
    all_to_all x2 -> x0, blocking collectives: 133 us -> none  [exchange_in_groups(): lax.all_to_all(group, axis, split_axis=split_dim, concat_axis=concat_dim,...]
    all_gather x4, waiting for transfers between devices: 105 us -> 51 us  [the longest x1 51 us: local(): up = lax.all_gather(up_weight_experts[0], 'tp')]
    reshape x13 -> x0, local copies, waits for them, and re-layouts: 50.9 us -> none  [the longest x2 12.8 us: expert_part(): flat = incoming.reshape(-1, incoming.shape[-1])]
    all_gather x2 -> x0, blocking collectives: 24.5 us -> none  [prefix_by_axis(): pieces = jax.tree.map(lambda part: lax.all_gather(part, axis), so_far)]
    all_to_all x5 -> x1, starting transfers between devices: 28.5 us -> 4.12 us  [local(): lax.all_to_all(shares, 'tp', split_axis=0, concat_axis=0, tiled=True)]
  transfers between devices with their start and end apart: 9 -> 5, of which waited for: 7 -> 2; matrix products, arithmetic and copies ran while one was open for 14% -> 2% of each run, Pallas kernels for 0% -> 52%
where the time goes in v1:
time: 393 us
  Pallas kernels  298 us (76%)
  waiting for transfers between devices  59.4 us (15%)
  between operations  13.3 us (3%)
  local copies, waits for them, and re-layouts  11 us (3%)
  matrix products  6.14 us (2%)
  starting transfers between devices  4.37 us (1%)
    pallas_call x2, Pallas kernels, exchange(): pl.pallas_call(functools.partial(exchange_kernel, n), name=f'exchange_{nu...  174 us
    pallas_call x1, Pallas kernels, mixer_local(): pl.pallas_call(functools.partial(mixer_kernel, pairs, chunks), name='mixe...  58.8 us
    all_gather x1, waiting for transfers between devices, local(): up = lax.all_gather(up_weight_experts[0], 'tp')  51 us
    pallas_call x1, Pallas kernels, prefix_states(): pl.pallas_call(functools.partial(prefix_kernel, n, pairs), name='prefix_s...  40.9 us
    unnamed x37, local copies, waits for them, and re-layouts  11 us
    pallas_call x1, Pallas kernels, expert_rows(): pl.pallas_call(functools.partial(expert_kernel, n, capacity), name='exper...  8.54 us
    pallas_call x1, Pallas kernels, readout(): pl.pallas_call(functools.partial(readout_kernel, width // LANES, length),...  8 us
  transfers between devices with their start and end apart: 5, of which 2 were waited for; matrix products, arithmetic and copies ran while one was open for 2% of the time, Pallas kernels for 52%

profile of v1, /device:TPU:33, one launch (start us, length us, event | category | flops | bytes accessed | tf_op | source)
XLA Modules:
  0.0 392.5 jit_solution(6313398869151379016)
XLA Ops:
  6.5 0.0 copy-start.14
  6.6 0.0 copy-start.5
  6.6 0.0 copy-start.9
  6.6 0.0 copy-start.10
  6.6 0.1 all-gather.12.cloned.1.call-start
  6.7 0.7 all-gather.12.cloned.1.call-update
  7.4 0.1 all-gather.10.cloned.1.call-start
  7.5 0.7 all-gather.10.cloned.1.call-update
  8.2 0.1 all-gather.6.cloned.1.call-start
  8.3 0.7 all-gather.6.cloned.1.call-update
  9.0 0.1 all-gather.8.cloned.1.call-start
  9.1 0.6 all-gather.8.cloned.1.call-update
  9.6 0.0 copy-done.14
  9.6 0.1 copy.24.offset_ref
  9.8 0.0 copy-done.11
  9.8 0.0 copy-done.12
  9.8 0.0 copy-done.3
  9.8 0.0 copy-done.4
  9.8 0.0 copy-done.5
  9.8 0.0 copy-done.9
  9.8 0.0 copy-done.10
  9.8 58.8 %mixer_local.1 = (bf16[4,2,64,128]{3,2,1,0:T(8,128)(2,1)S(1)}, bf16[512,512]{1,0:T(8,128)(2,1)S(1)}, f32[512,512]{1,0:T(8,128)S(1)}) custom-call(bf16[512,512]{1,0:T(8,128)(2,1)S(1)} %copy-done.3, bf16[512,512]{1,0:T(8,128)(2,1)S(1)} %copy-done.4, bf16[512,512]{1,0:T(8,128)(2,1)S(1)} %copy-done.5, bf16[512,512]{1,0:T(8,128)(2,1)S(1)} %copy-done.9, ...), custom_call_target="tpu_custom_call" | custom-call | flops 5368709120 | bytes 3145728 | tf_op jit(solution)/shard_map/mixer_local/pallas_call | solution.py:221
  68.7 0.0 copy-start.2
  68.7 1.0 copy-done.2
  69.7 0.8 copy-done.6
  70.5 0.7 copy-done.13
  71.2 40.9 %prefix_states.1.enter_ref = bf16[4,64,128]{2,1,0:T(8,128)(2,1)} custom-call(bf16[4,2,64,128]{3,2,1,0:T(8,128)(2,1)} %copy-done.13), custom_call_target="tpu_custom_call" | custom-call | flops 1000000000 | bytes 62914560 | tf_op jit(solution)/shard_map/prefix_states/pallas_call | solution.py:347
  112.1 8.0 %readout.1 = bf16[512,512]{1,0:T(8,128)(2,1)} custom-call(bf16[512,512]{1,0:T(8,128)(2,1)} %recept_ref.3, bf16[512,512]{1,0:T(8,128)(2,1)} %key_ref.3, bf16[512,512]{1,0:T(8,128)(2,1)} %value_ref.3, bf16[512,512]{1,0:T(8,128)(2,1)} %gate_ref.1, f32[1,512]{1,0:T(1,128)} %bitcast.17, f32[1,512]{1,0:T(1,128)} %bitcast.18, bf16[512,512]{1,0:T(8,128)(2,1)} %copy-done.6, ...), custom_call_target="tpu_custom_call" | custom-call | flops 1000000000 | bytes 16777216 | tf_op jit(solution)/shard_map/readout/pallas_call | solution.py:389
  120.1 4.1 %all-to-all-start = ((bf16[4,128,512]{2,1,0:T(8,128)(2,1)}), bf16[4,128,512]{2,1,0:T(8,128)(2,1)S(1)}, u32[]{:S(2)}, u32[]{:S(2)}) async-start(bf16[4,128,512]{2,1,0:T(8,128)(2,1)} %bitcast.16), calls=%async_computation | async-start | bytes 1048576 | tf_op jit(solution)/shard_map/all_to_all | solution.py:647
  124.2 0.0 copy-done.15
  124.2 0.7 copy.26.index_ref
  125.0 0.0 copy-done.16
  125.0 0.7 copy.27.weight_ref
  125.7 5.7 %all-to-all-done = bf16[4,128,512]{2,1,0:T(8,128)(2,1)S(1)} async-done(((bf16[4,128,512]{2,1,0:T(8,128)(2,1)}), bf16[4,128,512]{2,1,0:T(8,128)(2,1)S(1)}, u32[]{:S(2)}, u32[]{:S(2)}) %all-to-all-start) | async-done | bytes 524320 | tf_op jit(solution)/shard_map/all_to_all | solution.py:647
  131.3 6.1 %fusion.proj_ref = bf16[128,2048]{1,0:T(8,128)(2,1)} fusion(bf16[4,128,512]{2,1,0:T(8,128)(2,1)S(1)} %all-to-all-done, bf16[4,512,2048]{2,1,0:T(8,128)(2,1)} %bitcast.15), kind=kOutput, calls=%fused_computation.1 | convolution fusion | flops 1074003968 | bytes 9437184 | tf_op jit(solution)/shard_map/jrc,jcd->rd/dot_general | solution.py:648
  137.5 3.8 build.1.src_ref
  141.3 90.8 %exchange_1.1.came_ref = bf16[32,48,512]{2,1,0:T(8,128)(2,1)} custom-call(bf16[32,48,512]{2,1,0:T(8,128)(2,1)} %build.1.src_ref), custom_call_target="tpu_custom_call" | custom-call | flops 1000000 | bytes 209715200 | tf_op jit(solution)/shard_map/exchange_1/pallas_call | solution.py:499
  232.1 0.0 all-gather.10.cloned.1.call-done.down_ref
  232.1 0.0 all-gather.6.cloned.1.call-done.gate_ref
  232.2 51.0 %all-gather.8.cloned.1.call-done.up_ref = bf16[4,2048,256]{2,1,0:T(8,128)(2,1)} async-done(((bf16[1,2048,256]{2,1,0:T(8,128)(2,1)}), bf16[4,2048,256]{2,1,0:T(8,128)(2,1)}) %all-gather.8.cloned.1.call-update) | async-done | bytes 4194320 | tf_op jit(solution)/shard_map/all_gather | solution.py:634
  283.1 1.4 copy-done
  284.5 2.2 copy-done.7
  286.7 2.2 copy-done.8
  288.9 8.5 %expert_rows.1.src_ref = bf16[32,48,512]{2,1,0:T(8,128)(2,1)S(1)} custom-call(bf16[32,48,512]{2,1,0:T(8,128)(2,1)S(1)} %copy-done, bf16[4,2048,256]{2,1,0:T(8,128)(2,1)S(1)} %copy-done.7, bf16[4,2048,256]{2,1,0:T(8,128)(2,1)S(1)} %copy-done.8, bf16[4,256,2048]{2,1,0:T(8,128)(2,1)} %all-gather.10.cloned.1.call-done.down_ref), custom_call_target="tpu_custom_call" | custom-call | flops 5000000000 | bytes 16777216 | tf_op jit(solution)/shard_map/expert_rows/pallas_call | solution.py:564
  297.5 0.0 copy-start.1
  297.5 1.1 copy-done.1
  298.6 83.4 %exchange_2.1.back_ref = bf16[32,48,512]{2,1,0:T(8,128)(2,1)} custom-call(bf16[32,48,512]{2,1,0:T(8,128)(2,1)} %copy-done.1), custom_call_target="tpu_custom_call" | custom-call | flops 1000000 | bytes 209715200 | tf_op jit(solution)/shard_map/exchange_2/pallas_call | solution.py:499
  382.0 4.0 %combine.1 = bf16[128,2048]{1,0:T(8,128)(2,1)} custom-call(bf16[128,2048]{1,0:T(8,128)(2,1)} %residual_ref.3, bf16[128,2048]{1,0:T(8,128)(2,1)} %fusion.proj_ref, s32[128,2]{1,0:T(8,128)} %copy.26.index_ref, f32[128,2]{1,0:T(8,128)} %copy.27.weight_ref, bf16[32,48,512]{2,1,0:T(8,128)(2,1)} %exchange_2.1.back_ref), custom_call_target="tpu_custom_call" | custom-call | flops 1000000000 | bytes 8388608 | tf_op jit(solution)/shard_map/combine/pallas_call | solution.py:614
  (12 shorter events, 0.0 us)
Async XLA Ops:
  6.5 3.1 copy-start.14
  6.5 3.2 copy-start.11
  6.6 3.2 copy-start.12
  6.6 3.2 copy-start.3
  6.6 3.2 copy-start.4
  6.6 3.2 copy-start.5
  6.6 3.2 copy-start.9
  6.6 3.2 copy-start.10
  6.6 124.7 %all-gather.12.cloned.1.call-start = ((), (), s32[]{:S(2)}) async-start(), calls=%async_computation.4 | async-start | bytes 10485760 | tf_op jit(solution)/shard_map/all_gather | solution.py:632
  7.4 224.7 %all-gather.10.cloned.1.call-start = ((), (), s32[]{:S(2)}) async-start(), calls=%async_computation.3 | async-start | bytes 5242880 | tf_op jit(solution)/shard_map/all_gather | solution.py:635
  8.2 224.0 %all-gather.6.cloned.1.call-start = ((), (), s32[]{:S(2)}) async-start(), calls=%async_computation.1 | async-start | bytes 5242880 | tf_op jit(solution)/shard_map/all_gather | solution.py:633
  9.0 274.1 %all-gather.8.cloned.1.call-start = ((), (), s32[]{:S(2)}) async-start(), calls=%async_computation.2 | async-start | bytes 5242880 | tf_op jit(solution)/shard_map/all_gather | solution.py:634
  68.7 1.0 copy-start.2
  69.7 0.8 copy-start.6
  70.5 0.7 copy-start.13
  71.2 53.1 %copy-start.15 = (s32[128,2]{0,1:T(2,128)S(1)}, s32[128,2]{0,1:T(2,128)}, u32[]{:S(2)}) copy-start(s32[128,2]{0,1:T(2,128)} %param.33) | copy-start | bytes 3076
  71.2 53.8 %copy-start.16 = (f32[128,2]{0,1:T(2,128)S(1)}, f32[128,2]{0,1:T(2,128)}, u32[]{:S(2)}) copy-start(f32[128,2]{0,1:T(2,128)} %param.34) | copy-start | bytes 3076
  120.1 11.2 %all-to-all-start = ((bf16[4,128,512]{2,1,0:T(8,128)(2,1)}), bf16[4,128,512]{2,1,0:T(8,128)(2,1)S(1)}, u32[]{:S(2)}, u32[]{:S(2)}) async-start(bf16[4,128,512]{2,1,0:T(8,128)(2,1)} %bitcast.16), calls=%async_computation | async-start | bytes 1048576 | tf_op jit(solution)/shard_map/all_to_all | solution.py:647
  283.1 1.4 copy-start
  284.5 2.2 copy-start.7
  286.7 2.2 copy-start.8
  297.5 1.2 copy-start.1
Sparse Core Ops, SparseCore 0:
  9.3 104.0 all-gather.11
  115.2 55.0 all-gather.9
  172.1 54.6 all-gather.5
  228.4 54.6 all-gather.7

commit v2 on v1

--- a/solution.py
+++ b/solution.py
@@ -60,58 +60,78 @@
     return jnp.concatenate([jnp.where(first, x, zero), jnp.where(first, zero, x)], axis=0)
 
 
-def chunk_maps(recept, key, value, decay_pre, rate_pre, offset, decay_bias, rate_bias):
+def chunk_maps(units):
     row = iota((SPAN, LANES), 0)
     col = iota((SPAN, LANES), 1) & (HEAD - 1)
-    decay_log = offset - DECAY_SCALE * sigmoid(decay_bias + decay_pre)
-    rate = sigmoid(rate_bias + rate_pre)
-    norm = dot_split_left(key * key, head_ones())
-    unit = key * lax.rsqrt(norm + NORM_EPS)
     square = (SPAN, SPAN)
     lower = jnp.where(iota(square, 0) >= iota(square, 1), 1.0, 0.0).astype(bf16)
-    cumul = dot_split_right(lower, decay_log)
-    middle = cumul[SPAN // 2 - 1 : SPAN // 2, :]
-    rel = cumul - middle
-    rise, fall = jnp.exp(rel), jnp.exp(-rel)
-    to_middle = jnp.exp(middle)
-    to_end = jnp.exp(cumul[SPAN - 1 : SPAN, :] - middle)
-    remove = -unit * jnp.exp(rel - decay_log)
-    read = recept * rise
-    write = unit * rate * fall
-    keys = key * fall
-    scores = dot(
-        jnp.concatenate([remove.astype(bf16), read.astype(bf16)], axis=0),
-        jnp.concatenate([stacked(write.astype(bf16)), stacked(keys.astype(bf16))], axis=0),
-        NT,
-    )
+    ones = head_ones()
+
+    def each(work, *lists):
+        return [work(*parts) for parts in zip(*lists)]
+
+    def elementwise(recept, key, value, decay_pre, rate_pre, offset, decay_bias, rate_bias):
+        decay_log = offset - DECAY_SCALE * sigmoid(decay_bias + decay_pre.astype(f32))
+        key = key.astype(f32)
+        return decay_log, dot_split_right(lower, decay_log), dot_split_left(key * key, ones)
+
+    def scaled(unit, first):
+        recept, key, value, decay_pre, rate_pre, offset, decay_bias, rate_bias = unit
+        decay_log, cumul, norm = first
+        key = key.astype(f32)
+        rate = sigmoid(rate_bias + rate_pre.astype(f32))
+        unit_key = key * lax.rsqrt(norm + NORM_EPS)
+        middle = cumul[SPAN // 2 - 1 : SPAN // 2, :]
+        rel = cumul - middle
+        rise, fall = jnp.exp(rel), jnp.exp(-rel)
+        to_middle = jnp.exp(middle)
+        to_end = jnp.exp(cumul[SPAN - 1 : SPAN, :] - middle)
+        remove = -unit_key * jnp.exp(rel - decay_log)
+        read = recept.astype(f32) * rise
+        write = unit_key * rate * fall
+        keys = key * fall
+        left = jnp.concatenate([remove.astype(bf16), read.astype(bf16)], axis=0)
+        right = jnp.concatenate([stacked(write.astype(bf16)), stacked(keys.astype(bf16))], axis=0)
+        from_start = [(remove * to_middle).astype(bf16), (read * to_middle).astype(bf16)]
+        write_end = jnp.concatenate([write * to_end, keys * to_end], axis=0).T.astype(bf16)
+        ending = jnp.broadcast_to(to_end * to_middle, (LANES, LANES)).T
+        return dot(left, right, NT), from_start, write_end, ending
+
+    first = [elementwise(*unit) for unit in units]
+    second = each(scaled, units, first)
+    scores = [item[0] for item in second]
     strict, within = row > col, row >= col
-    lower_part = jnp.where(strict, scores[:SPAN, :LANES], 0.0)
-    remove_key = jnp.where(strict, scores[:SPAN, LANES:], 0.0)
-    read_write = jnp.where(within, scores[SPAN:, :LANES], 0.0)
-    read_key = jnp.where(within, scores[SPAN:, LANES:], 0.0)
 
     def merging(level):
         size = 1 << level
         same = (row >> (level + 1)) == (col >> (level + 1))
         return same & ((row & size) != 0) & ((col & size) == 0)
 
-    inverse = jnp.where(row == col, 1.0, jnp.where(merging(0), lower_part, 0.0))
+    lower_part = [jnp.where(strict, s[:SPAN, :LANES], 0.0).astype(bf16) for s in scores]
+    remove_key = [jnp.where(strict, s[:SPAN, LANES:], 0.0).astype(bf16) for s in scores]
+    within_maps = [
+        jnp.where(
+            jnp.concatenate([within, within], axis=1), s[SPAN:], 0.0
+        ).astype(bf16)
+        for s in scores
+    ]
+    removed_value = [dot(m, stacked(unit[2])).astype(bf16) for m, unit in zip(remove_key, units)]
+    inverse = [jnp.where(row == col, 1.0, jnp.where(merging(0), m.astype(f32), 0.0)) for m in lower_part]
     for level in range(1, SPAN.bit_length() - 1):
-        block = jnp.where(merging(level), lower_part, 0.0)
-        inner = dot(block, stacked(inverse.astype(bf16)))
-        inverse = inverse + dot(inverse, stacked(inner.astype(bf16)))
-    removed_value = dot(remove_key, stacked(value.astype(bf16)))
-    solved = dot(
-        inverse,
-        jnp.concatenate(
-            [stacked((remove * to_middle).astype(bf16)), stacked(removed_value.astype(bf16))], axis=1
-        ),
-    )
-    left = jnp.concatenate([solved[:, :LANES], read * to_middle], axis=0).astype(bf16)
-    write_end = jnp.concatenate([write * to_end, keys * to_end], axis=0).T.astype(bf16)
-    ending = jnp.broadcast_to(to_end * to_middle, (LANES, LANES)).T
-    within_maps = jnp.concatenate([read_write, read_key], axis=1).astype(bf16)
-    return left, solved[:, LANES:], within_maps, write_end, ending
+        chosen = merging(level)
+        inner = [
+            dot(jnp.where(chosen, m, jnp.zeros_like(m)), stacked(x.astype(bf16)))
+            for m, x in zip(lower_part, inverse)
+        ]
+        inverse = [x + dot(x, stacked(y.astype(bf16))) for x, y in zip(inverse, inner)]
+    solved = [
+        dot(x, jnp.concatenate([stacked(item[1][0]), stacked(v)], axis=1))
+        for x, item, v in zip(inverse, second, removed_value)
+    ]
+    return [
+        (jnp.concatenate([q[:, :LANES].astype(bf16), item[1][1]], axis=0), q[:, LANES:], maps) + item[2:]
+        for q, item, maps in zip(solved, second, within_maps)
+    ]
 
 
 def mixer_kernel(
@@ -125,37 +145,32 @@
     def rows_of(c):
         return pl.ds(pl.multiple_of(c * SPAN, SPAN), SPAN)
 
-    def prepare(c):
-        rows = rows_of(c)
-        for p in range(pairs):
-            cols = slice(p * LANES, (p + 1) * LANES)
+    unroll = 2 if chunks % 2 == 0 else 1
+
+    def prepare(i, _):
+        places = [(i * unroll + k, p) for k in range(unroll) for p in range(pairs)]
+        units = []
+        for c, p in places:
+            rows, cols = rows_of(c), slice(p * LANES, (p + 1) * LANES)
             offset = jnp.where(
                 first_head, offset_ref[rows, 2 * p : 2 * p + 1], offset_ref[rows, 2 * p + 1 : 2 * p + 2]
             )
-            left, solved, within, write, ending = chunk_maps(
-                recept_ref[rows, cols].astype(f32),
-                key_ref[rows, cols].astype(f32),
-                value_ref[rows, cols].astype(f32),
-                decay_ref[rows, cols].astype(f32),
-                rate_ref[rows, cols].astype(f32),
-                offset,
-                decay_bias_ref[:, cols],
-                rate_bias_ref[:, cols],
+            units.append(
+                (
+                    recept_ref[rows, cols], key_ref[rows, cols], value_ref[rows, cols],
+                    decay_ref[rows, cols], rate_ref[rows, cols], offset,
+                    decay_bias_ref[:, cols], rate_bias_ref[:, cols],
+                )
             )
+        for (c, p), (left, solved, within, write, ending) in zip(places, chunk_maps(units)):
             left_ref[c, p] = left
             solved_ref[c, p] = solved
             within_ref[c, p] = within
             write_ref[c, p] = write
             ending_ref[c, p] = ending
-
-    unroll = 2 if chunks % 2 == 0 else 1
-
-    def prepare_some(i, _):
-        for k in range(unroll):
-            prepare(i * unroll + k)
         return 0
 
-    lax.fori_loop(0, chunks // unroll, prepare_some, 0)
+    lax.fori_loop(0, chunks // unroll, prepare, 0)
 
     square = (LANES, LANES)
     eye = jnp.where(iota(square, 0) == iota(square, 1), 1.0, 0.0)
@@ -166,22 +181,27 @@
 
     def advance(c, _):
         rows = rows_of(c)
+        states = [state_ref[p] for p in range(pairs)]
+        crossed = [dot(left_ref[c, p], states[p]) for p in range(pairs)]
+        removed = [
+            jnp.concatenate(
+                [x[:SPAN, :LANES], x[:SPAN, LANES:] + solved_ref[c, p]], axis=1
+            ).astype(bf16)
+            for p, x in enumerate(crossed)
+        ]
+        updates = []
         for p in range(pairs):
             value = value_ref[rows, p * LANES : (p + 1) * LANES]
-            state = state_ref[p]
-            crossed = dot(left_ref[c, p], state)
-            removed = jnp.concatenate(
-                [crossed[:SPAN, :LANES], crossed[:SPAN, LANES:] + solved_ref[c, p]], axis=1
-            ).astype(bf16)
-            removed_ref[c, p] = removed
-            partial_ref[c, p] = crossed[SPAN:]
             right = jnp.concatenate(
-                [removed, jnp.concatenate([jnp.zeros_like(value), value], axis=1)], axis=0
+                [removed[p], jnp.concatenate([jnp.zeros_like(value), value], axis=1)], axis=0
             )
-            update = dot(write_ref[c, p], right)
+            updates.append(dot(write_ref[c, p], right))
+        for p in range(pairs):
+            removed_ref[c, p] = removed[p]
+            partial_ref[c, p] = crossed[p][SPAN:]
             ending = ending_ref[c, p]
-            state_ref[p] = state * jnp.concatenate([ending, ending], axis=1) + jnp.where(
-                own_block, update, 0.0
+            state_ref[p] = states[p] * jnp.concatenate([ending, ending], axis=1) + jnp.where(
+                own_block, updates[p], 0.0
             )
         return 0
 
@@ -238,7 +258,6 @@
             pltpu.VMEM(per + (SPAN, 2 * LANES), bf16),
             pltpu.VMEM(per + (SPAN, 2 * LANES), f32),
         ],
-        compiler_params=pltpu.CompilerParams(vmem_limit_bytes=40 << 20),
         cost_estimate=pl.CostEstimate(
             flops=80 * 2 * LANES * length * width, bytes_accessed=12 * length * width, transcendentals=0
         ),
@@ -411,7 +430,8 @@
 def build_kernel(experts, capacity, residual_ref, proj_ref, gain_ref, index_ref, out_ref, stack_ref):
     rows, width = residual_ref.shape
     part = width // QUARTERS
-    stream = residual_ref[...].astype(f32) + proj_ref[...].astype(f32)
+    proj = jnp.concatenate([proj_ref[0], proj_ref[1]], axis=1)
+    stream = residual_ref[...].astype(f32) + proj.astype(f32)
     scale = lax.rsqrt(jnp.mean(stream * stream, axis=1, keepdims=True) + NORM_EPS)
     ffn_in = (stream * scale * gain_ref[...]).astype(bf16)
     for q in range(QUARTERS):
@@ -495,6 +515,251 @@
     lax.fori_loop(1, n, finish, 0)
 
 
+def other_core(me):
+    return me + 1 - 2 * lax.rem(me, 2)
+
+
+def spread_kernel(m, src_ref, out_ref, own_sem, sent, came, pass_sent, pass_came):
+    me, col = lax.axis_index("sp"), lax.axis_index("tp")
+    core, partner = lax.rem(me, 2), other_core(me)
+    barrier = pltpu.get_barrier_semaphore()
+    pl.semaphore_signal(barrier, inc=1, device_id={"sp": partner}, device_id_type=MESH)
+    for k in range(1, m):
+        pl.semaphore_signal(
+            barrier, inc=1, device_id={"tp": lax.rem(col + k, m)}, device_id_type=MESH
+        )
+    own = pltpu.make_async_copy(src_ref.at[col], out_ref.at[core, col], own_sem)
+    own.start()
+    pl.semaphore_wait(barrier, m)
+
+    def send(k):
+        to = lax.rem(col + k, m)
+        return pltpu.make_async_remote_copy(
+            src_ref=src_ref.at[to], dst_ref=out_ref.at[core, col], send_sem=sent.at[k],
+            recv_sem=came.at[k], device_id={"tp": to}, device_id_type=MESH,
+        )
+
+    def arrival(k):
+        frm = lax.rem(col + m - k, m)
+        return pltpu.make_async_remote_copy(
+            src_ref=src_ref.at[frm], dst_ref=out_ref.at[core, frm], send_sem=sent.at[k],
+            recv_sem=came.at[k], device_id={"tp": frm}, device_id_type=MESH,
+        )
+
+    def onward(k, source):
+        frm = lax.rem(col + m - k, m)
+        return pltpu.make_async_remote_copy(
+            src_ref=source, dst_ref=out_ref.at[core, frm], send_sem=pass_sent.at[k],
+            recv_sem=pass_came.at[k], device_id={"sp": partner}, device_id_type=MESH,
+        )
+
+    def from_partner(k):
+        frm = lax.rem(col + m - k, m)
+        return pltpu.make_async_remote_copy(
+            src_ref=src_ref.at[frm], dst_ref=out_ref.at[1 - core, frm], send_sem=pass_sent.at[k],
+            recv_sem=pass_came.at[k], device_id={"sp": partner}, device_id_type=MESH,
+        )
+
+    order = [m // 2] + [k for k in range(1, m) if k != m // 2]
+    for k in order:
+        send(k).start()
+    onward(0, src_ref.at[col]).start()
+    passed = [k for k in range(1, m) if k != m // 2] + [m // 2]
+    for k in passed:
+        arrival(k).wait_recv()
+        onward(k, out_ref.at[core, lax.rem(col + m - k, m)]).start()
+    own.wait()
+    for k in range(m):
+        from_partner(k).wait_recv()
+        onward(k, src_ref.at[col]).wait_send()
+    for k in range(1, m):
+        send(k).wait_send()
+
+
+def spread(blocks, m, number):
+    return pl.pallas_call(
+        functools.partial(spread_kernel, m),
+        name="spread",
+        out_shape=jax.ShapeDtypeStruct((2,) + blocks.shape, blocks.dtype),
+        in_specs=[VMEM_SPEC],
+        out_specs=VMEM_SPEC,
+        scratch_shapes=[pltpu.SemaphoreType.DMA] + [pltpu.SemaphoreType.DMA((m,))] * 4,
+        compiler_params=pltpu.CompilerParams(collective_id=number, has_side_effects=True),
+        cost_estimate=pl.CostEstimate(flops=10**6, bytes_accessed=40 << 20, transcendentals=0),
+    )(blocks)
+
+
+def swap_kernel(src_ref, out_ref, own_sem, sent, came):
+    me = lax.axis_index("sp")
+    core, partner = lax.rem(me, 2), other_core(me)
+    barrier = pltpu.get_barrier_semaphore()
+    pl.semaphore_signal(barrier, inc=1, device_id={"sp": partner}, device_id_type=MESH)
+    own = pltpu.make_async_copy(src_ref.at[core], out_ref.at[core], own_sem)
+    own.start()
+    pl.semaphore_wait(barrier, 1)
+    away = pltpu.make_async_remote_copy(
+        src_ref=src_ref.at[1 - core], dst_ref=out_ref.at[core], send_sem=sent, recv_sem=came,
+        device_id={"sp": partner}, device_id_type=MESH,
+    )
+    away.start()
+    own.wait()
+    pltpu.make_async_remote_copy(
+        src_ref=src_ref.at[1 - core], dst_ref=out_ref.at[1 - core], send_sem=sent, recv_sem=came,
+        device_id={"sp": partner}, device_id_type=MESH,
+    ).wait_recv()
+    away.wait_send()
+
+
+def swap(blocks, number):
+    return pl.pallas_call(
+        swap_kernel,
+        name="swap",
+        out_shape=jax.ShapeDtypeStruct(blocks.shape, blocks.dtype),
+        in_specs=[VMEM_SPEC],
+        out_specs=VMEM_SPEC,
+        scratch_shapes=[pltpu.SemaphoreType.DMA] * 3,
+        compiler_params=pltpu.CompilerParams(collective_id=number, has_side_effects=True),
+        cost_estimate=pl.CostEstimate(flops=10**6, bytes_accessed=4 << 20, transcendentals=0),
+    )(blocks)
+
+
+def exchange_gather_kernel(n, m, src_ref, first_ref, second_ref, out_ref, first_all, second_all,
+                           stage, own_sem, sent, came, in_sem, out_sem, ring_sent, ring_came, pass_sent, pass_came):
+    me, col = lax.axis_index("sp"), lax.axis_index("tp")
+    right, left = lax.rem(col + 1, m), lax.rem(col + m - 1, m)
+    shards, wholes = (first_ref, second_ref), (first_all, second_all)
+    barrier = pltpu.get_barrier_semaphore()
+
+    def greet(k, _):
+        pl.semaphore_signal(
+            barrier, inc=1, device_id={"sp": lax.rem(me + k, n)}, device_id_type=MESH
+        )
+        return 0
+
+    for side in (left, right):
+        pl.semaphore_signal(barrier, inc=1, device_id={"tp": side}, device_id_type=MESH)
+    lax.fori_loop(1, n, greet, 0)
+    own = pltpu.make_async_copy(src_ref.at[me], out_ref.at[me], own_sem)
+    own.start()
+    loads = [pltpu.make_async_copy(shards[a], stage.at[a], in_sem.at[a]) for a in range(2)]
+    stores = [pltpu.make_async_copy(stage.at[a], wholes[a].at[col], out_sem.at[a]) for a in range(2)]
+    for load in loads:
+        load.start()
+    for load in loads:
+        load.wait()
+    pl.semaphore_wait(barrier, n + 1)
+
+    def copy(k):
+        to = lax.rem(me + k, n)
+        return pltpu.make_async_remote_copy(
+            src_ref=src_ref.at[to], dst_ref=out_ref.at[me], send_sem=sent.at[k], recv_sem=came.at[k],
+            device_id={"sp": to}, device_id_type=MESH,
+        )
+
+    def start(k, _):
+        away = n // 2 - lax.div(k, 2)
+        copy(jnp.where(lax.rem(k, 2) == 0, away, n - away)).start()
+        return 0
+
+    def arrived(k):
+        frm = lax.rem(me + n - k, n)
+        return pltpu.make_async_remote_copy(
+            src_ref=src_ref.at[frm], dst_ref=out_ref.at[frm], send_sem=sent.at[k], recv_sem=came.at[k],
+            device_id={"sp": frm}, device_id_type=MESH,
+        )
+
+    half = first_ref.shape[0] // 2
+
+    def rows(h):
+        return pl.ds(h * half, half)
+
+    def hop(a, d, h):
+        return pltpu.make_async_remote_copy(
+            src_ref=stage.at[a, rows(h)], dst_ref=wholes[a].at[col, rows(h)],
+            send_sem=ring_sent.at[a, d, h], recv_sem=ring_came.at[a, d, h],
+            device_id={"tp": (right, left)[d]}, device_id_type=MESH,
+        )
+
+    def hop_in(a, d, h):
+        frm = (left, right)[d]
+        return pltpu.make_async_remote_copy(
+            src_ref=stage.at[a, rows(h)], dst_ref=wholes[a].at[frm, rows(h)],
+            send_sem=ring_sent.at[a, d, h], recv_sem=ring_came.at[a, d, h],
+            device_id={"tp": frm}, device_id_type=MESH,
+        )
+
+    def onward(a, d):
+        frm = (left, right)[d]
+        return pltpu.make_async_remote_copy(
+            src_ref=wholes[a].at[frm, rows(d)], dst_ref=wholes[a].at[frm, rows(d)],
+            send_sem=pass_sent.at[a, d], recv_sem=pass_came.at[a, d],
+            device_id={"tp": (right, left)[d]}, device_id_type=MESH,
+        )
+
+    def onward_in(a, d):
+        frm = lax.rem(col + 2, m)
+        return pltpu.make_async_remote_copy(
+            src_ref=wholes[a].at[frm, rows(d)], dst_ref=wholes[a].at[frm, rows(d)],
+            send_sem=pass_sent.at[a, d], recv_sem=pass_came.at[a, d],
+            device_id={"tp": (left, right)[d]}, device_id_type=MESH,
+        )
+
+    copy(n // 2).start()
+    lax.fori_loop(2, n, start, 0)
+    for a in range(2):
+        for d, h in ((0, 0), (1, 1), (0, 1), (1, 0)):
+            hop(a, d, h).start()
+    for store in stores:
+        store.start()
+    for a in range(2):
+        for d in range(2):
+            hop_in(a, d, d).wait_recv()
+            onward(a, d).start()
+    own.wait()
+    for store in stores:
+        store.wait()
+
+    def finish(k, _):
+        arrived(k).wait_recv()
+        copy(k).wait_send()
+        return 0
+
+    lax.fori_loop(1, n, finish, 0)
+    for a in range(2):
+        for d in range(2):
+            hop_in(a, d, 1 - d).wait_recv()
+            onward_in(a, d).wait_recv()
+            onward(a, d).wait_send()
+            for h in range(2):
+                hop(a, d, h).wait_send()
+
+
+def exchange_and_gather(blocks, first, second, n, m, number):
+    any_spec = pl.BlockSpec(memory_space=pl.ANY)
+    whole = jax.ShapeDtypeStruct((m,) + first.shape, first.dtype)
+    return pl.pallas_call(
+        functools.partial(exchange_gather_kernel, n, m),
+        name=f"exchange_{number}",
+        out_shape=(jax.ShapeDtypeStruct(blocks.shape, blocks.dtype), whole, whole),
+        in_specs=[VMEM_SPEC, any_spec, any_spec],
+        out_specs=(VMEM_SPEC, any_spec, any_spec),
+        scratch_shapes=[
+            pltpu.VMEM((2,) + first.shape, first.dtype),
+            pltpu.SemaphoreType.DMA,
+            pltpu.SemaphoreType.DMA((n,)),
+            pltpu.SemaphoreType.DMA((n,)),
+            pltpu.SemaphoreType.DMA((2,)),
+            pltpu.SemaphoreType.DMA((2,)),
+            pltpu.SemaphoreType.DMA((2, 2, 2)),
+            pltpu.SemaphoreType.DMA((2, 2, 2)),
+            pltpu.SemaphoreType.DMA((2, 2)),
+            pltpu.SemaphoreType.DMA((2, 2)),
+        ],
+        compiler_params=pltpu.CompilerParams(collective_id=number, has_side_effects=True),
+        cost_estimate=pl.CostEstimate(flops=10**6, bytes_accessed=200 << 20, transcendentals=0),
+    )(blocks, first, second)
+
+
 def exchange(blocks, n, number):
     return pl.pallas_call(
         functools.partial(exchange_kernel, n),
@@ -577,9 +842,7 @@
             pltpu.VMEM((n * capacity, width), bf16),
             pltpu.VMEM((n * capacity, width), f32),
         ],
-        compiler_params=pltpu.CompilerParams(
-            dimension_semantics=("arbitrary",), vmem_limit_bytes=40 << 20
-        ),
+        compiler_params=pltpu.CompilerParams(dimension_semantics=("arbitrary",)),
         cost_estimate=pl.CostEstimate(flops=5 * 10**9, bytes_accessed=16 << 20, transcendentals=0),
     )(came, gate, up, down)
 
@@ -605,7 +868,9 @@
     for q in range(QUARTERS):
         cols = slice(q * part, (q + 1) * part)
         routed = dot(high, rows_ref[:, cols]) + dot(low, rows_ref[:, cols])
-        stream = residual_ref[:, cols].astype(f32) + proj_ref[:, cols].astype(f32)
+        half, within = divmod(q, QUARTERS // 2)
+        proj = proj_ref[half, :, within * part : (within + 1) * part]
+        stream = residual_ref[:, cols].astype(f32) + proj.astype(f32)
         out_ref[:, cols] = (stream + routed).astype(bf16)
 
 
@@ -629,29 +894,36 @@
     gate_weight_experts, up_weight_experts, down_weight_experts,
 ):
     n = lax.axis_size("sp")
-    out_weight = lax.all_gather(output_weight_matrix, "tp")
-    gate = lax.all_gather(gate_weight_experts[0], "tp")
-    up = lax.all_gather(up_weight_experts[0], "tp")
-    down = lax.all_gather(down_weight_experts[0], "tp")
+    cores = 2
+    share = output_weight_matrix.shape[1] // cores
+    columns = lax.dynamic_slice_in_dim(
+        output_weight_matrix, lax.rem(lax.axis_index("sp"), cores) * share, share, axis=1
+    )
+    columns = lax.all_gather(columns, "tp")
 
     summary, maps, own = mixer_local(
         recept, key_input, value_input, decay_input_part, correction_rate_input, head_decay_offset,
         decay_fixed_bias[None], correction_rate_bias[None],
     )
     enter = prefix_states(summary, n)
+    down, enter = lax.optimization_barrier((down_weight_experts[0], enter))
+    down = lax.all_gather(down, "tp")
     mixed = readout(
         recept, key_input, value_input, output_gate_input, head_norm_gain[None], self_term_weight[None],
         maps, own, enter,
     )
-    shares = mixed.reshape(lax.axis_size("tp"), -1, mixed.shape[1])
-    shares = lax.all_to_all(shares, "tp", split_axis=0, concat_axis=0, tiled=True)
-    proj = jnp.einsum("jrc,jcd->rd", shares, out_weight, preferred_element_type=f32).astype(bf16)
+    m = lax.axis_size("tp")
+    shares = spread(mixed.reshape(m, -1, mixed.shape[1]), m, 3)
+    halves_of_proj = jnp.einsum("hjrc,jcd->hrd", shares, columns, preferred_element_type=f32)
+    proj = swap(halves_of_proj.astype(bf16), 4)
 
     rows = residual.shape[0]
     experts = gate_weight_experts.shape[0] * n
     capacity = 3 * rows // experts
     outgoing = build(residual, proj, feedforward_norm_gain[None], routed_expert_index, experts, capacity)
-    came = exchange(outgoing, n, 1)
+    came, gate, up = exchange_and_gather(
+        outgoing, gate_weight_experts[0], up_weight_experts[0], n, lax.axis_size("tp"), 1
+    )
     results = expert_rows(came, gate, up, down, capacity)
     back = exchange(results, n, 2)
     return combine(residual, proj, routed_expert_index, routed_expert_weight, back, capacity)

time: 393 us -> 310 us (0.79)
  waiting for transfers between devices: 59.4 us -> 0.15 us
  Pallas kernels: 298 us -> 285 us
  local copies, waits for them, and re-layouts: 11 us -> 5.78 us
  starting transfers between devices: 4.37 us -> 0.07 us
    pallas_call x0 -> x3, Pallas kernels: none -> 117 us  [the longest x1 98.6 us: exchange_and_gather(): pl.pallas_call(functools.partial(exchange_gather_kernel, n, m), name=f'ex...]
    pallas_call x2 -> x1, Pallas kernels: 174 us -> 83 us  [exchange(): pl.pallas_call(functools.partial(exchange_kernel, n), name=f'exchange_{nu...]
    all_gather x4 -> x2, waiting for transfers between devices: 51 us -> 0.04 us  [the longest x1 0.02 us: local(): columns = lax.all_gather(columns, 'tp')]
    pallas_call x1, Pallas kernels: 58.8 us -> 16.9 us  [mixer_local(): pl.pallas_call(functools.partial(mixer_kernel, pairs, chunks), name='mixe...]
    unnamed x37 -> x9, local copies, waits for them, and re-layouts: 11 us -> 4.62 us
    all_to_all x1 -> x0, waiting for transfers between devices: 5.65 us -> none  [local(): lax.all_to_all(shares, 'tp', split_axis=0, concat_axis=0, tiled=True)]
    all_to_all x1 -> x0, starting transfers between devices: 4.12 us -> none  [local(): lax.all_to_all(shares, 'tp', split_axis=0, concat_axis=0, tiled=True)]
  transfers between devices with their start and end apart: 5 -> 2, of which waited for: 2 -> 0; matrix products, arithmetic and copies ran while one was open for 2% -> 3% of each run, Pallas kernels for 52% -> 60%
where the time goes in v2:
time: 310 us
  Pallas kernels  285 us (92%)
  between operations  13.5 us (4%)
  local copies, waits for them, and re-layouts  5.78 us (2%)
  matrix products  4.74 us (2%)
    pallas_call x1, Pallas kernels, exchange_and_gather(): pl.pallas_call(functools.partial(exchange_gather_kernel, n, m), name=f'ex...  98.6 us
    pallas_call x1, Pallas kernels, exchange(): pl.pallas_call(functools.partial(exchange_kernel, n), name=f'exchange_{nu...  83 us
    pallas_call x1, Pallas kernels, prefix_states(): pl.pallas_call(functools.partial(prefix_kernel, n, pairs), name='prefix_s...  40.9 us
    pallas_call x1, Pallas kernels, mixer_local(): pl.pallas_call(functools.partial(mixer_kernel, pairs, chunks), name='mixe...  16.9 us
    pallas_call x1, Pallas kernels, spread(): pl.pallas_call(functools.partial(spread_kernel, m), name='spread', out_sh...  15.2 us
    pallas_call x1, Pallas kernels, expert_rows(): pl.pallas_call(functools.partial(expert_kernel, n, capacity), name='exper...  11.5 us
    pallas_call x1, Pallas kernels, readout(): pl.pallas_call(functools.partial(readout_kernel, width // LANES, length),...  7.99 us
  transfers between devices with their start and end apart: 2, of which 0 were waited for; matrix products, arithmetic and copies ran while one was open for 3% of the time, Pallas kernels for 60%

profile of v2, /device:TPU:33, one launch (start us, length us, event | category | flops | bytes accessed | tf_op | source)
XLA Modules:
  0.0 309.7 jit_solution(14305484493681881391)
XLA Ops:
  6.5 0.0 copy-start
  6.6 0.0 all-gather.5.cloned.1.call-start
  6.6 1.6 copy-done
  8.1 1.2 constant_dynamic-slice_fusion
  9.3 0.1 all-gather.5.cloned.1.call-update
  9.4 0.1 all-gather.7.cloned.1.call-start
  9.4 1.6 copy.20.offset_ref
  11.0 16.9 %mixer_local.1 = (bf16[4,2,64,128]{3,2,1,0:T(8,128)(2,1)}, bf16[512,512]{1,0:T(8,128)(2,1)}, f32[512,512]{1,0:T(8,128)}) custom-call(bf16[512,512]{1,0:T(8,128)(2,1)} %recept_ref.3, bf16[512,512]{1,0:T(8,128)(2,1)} %key_ref.3, bf16[512,512]{1,0:T(8,128)(2,1)} %value_ref.3, bf16[512,512]{1,0:T(8,128)(2,1)} %decay_ref.1, bf16[512,512]{1,0:T(8,128)(2,1)} %rate_ref.1, ...), custom_call_target="tpu_custom_call" | custom-call | flops 5368709120 | bytes 3145728 | tf_op jit(solution)/shard_map/mixer_local/pallas_call | solution.py:241
  27.9 0.0 copy-start.1
  27.9 0.0 copy-start.2
  27.9 40.9 %prefix_states.1.enter_ref = bf16[4,64,128]{2,1,0:T(8,128)(2,1)} custom-call(bf16[4,2,64,128]{3,2,1,0:T(8,128)(2,1)} %get-tuple-element.15.summary_ref), custom_call_target="tpu_custom_call" | custom-call | flops 1000000000 | bytes 62914560 | tf_op jit(solution)/shard_map/prefix_states/pallas_call | solution.py:366
  68.8 0.1 all-gather.7.cloned.1.call-update
  68.9 0.0 copy-done.1
  68.9 0.7 copy.22.index_ref
  69.7 0.0 copy-done.2
  69.7 0.7 copy.23.weight_ref
  70.4 8.0 %readout.1 = bf16[512,512]{1,0:T(8,128)(2,1)} custom-call(bf16[512,512]{1,0:T(8,128)(2,1)} %recept_ref.3, bf16[512,512]{1,0:T(8,128)(2,1)} %key_ref.3, bf16[512,512]{1,0:T(8,128)(2,1)} %value_ref.3, bf16[512,512]{1,0:T(8,128)(2,1)} %gate_ref.1, f32[1,512]{1,0:T(1,128)} %bitcast.24, f32[1,512]{1,0:T(1,128)} %bitcast.25, ...), custom_call_target="tpu_custom_call" | custom-call | flops 1000000000 | bytes 16777216 | tf_op jit(solution)/shard_map/readout/pallas_call | solution.py:408
  78.4 15.2 %spread.1 = bf16[2,4,128,512]{3,2,1,0:T(8,128)(2,1)} custom-call(bf16[4,128,512]{2,1,0:T(8,128)(2,1)} %bitcast.20), custom_call_target="tpu_custom_call" | custom-call | flops 1000000 | bytes 41943040 | tf_op jit(solution)/shard_map/spread/pallas_call | solution.py:580
  93.6 0.0 all-gather.5.cloned.1.call-done
  93.6 4.7 %fusion.src_ref = bf16[2,128,1024]{2,1,0:T(8,128)(2,1)} fusion(bf16[2,4,128,512]{3,2,1,0:T(8,128)(2,1)} %spread.1, bf16[4,512,1024,1]{2,1,0,3:T(8,128)(2,1)} %bitcast.26), kind=kOutput, calls=%fused_computation.1 | convolution fusion | flops 1074003968 | bytes 5767168 | tf_op jit(solution)/shard_map/hjrc,jcd->hrd/dot_general | solution.py:917
  98.4 3.5 %swap.1.proj_ref = bf16[2,128,1024]{2,1,0:T(8,128)(2,1)} custom-call(bf16[2,128,1024]{2,1,0:T(8,128)(2,1)} %fusion.src_ref), custom_call_target="tpu_custom_call" | custom-call | flops 1000000 | bytes 4194304 | tf_op jit(solution)/shard_map/swap/pallas_call | solution.py:614
  101.8 3.8 %build.1.src_ref = bf16[32,48,512]{2,1,0:T(8,128)(2,1)} custom-call(bf16[128,2048]{1,0:T(8,128)(2,1)} %residual_ref.3, bf16[2,128,1024]{2,1,0:T(8,128)(2,1)} %swap.1.proj_ref, f32[1,2048]{1,0:T(1,128)} %bitcast.28, s32[128,2]{1,0:T(8,128)} %copy.22.index_ref), custom_call_target="tpu_custom_call" | custom-call | flops 1000000000 | bytes 8388608 | tf_op jit(solution)/shard_map/build/pallas_call | solution.py:461
  105.6 98.6 %exchange_1.1 = (bf16[32,48,512]{2,1,0:T(8,128)(2,1)}, bf16[4,2048,256]{2,1,0:T(8,128)(2,1)}, bf16[4,2048,256]{2,1,0:T(8,128)(2,1)}) custom-call(bf16[32,48,512]{2,1,0:T(8,128)(2,1)} %build.1.src_ref, bf16[2048,256]{1,0:T(8,128)(2,1)} %bitcast.21, bf16[2048,256]{1,0:T(8,128)(2,1)} %bitcast.22), custom_call_target="tpu_custom_call" | custom-call | flops 1000000 | bytes 209715200 | tf_op jit(solution)/shard_map/exchange_1/pallas_call | solution.py:740
  204.3 0.0 all-gather.7.cloned.1.call-done
  204.3 11.5 %expert_rows.1.src_ref = bf16[32,48,512]{2,1,0:T(8,128)(2,1)} custom-call(bf16[32,48,512]{2,1,0:T(8,128)(2,1)} %get-tuple-element.17.came_ref, bf16[4,2048,256]{2,1,0:T(8,128)(2,1)} %get-tuple-element.18.gate_ref, bf16[4,2048,256]{2,1,0:T(8,128)(2,1)} %get-tuple-element.19.up_ref, bf16[4,256,2048]{2,1,0:T(8,128)(2,1)} %bitcast.27), custom_call_target="tpu_custom_call" | custom-call | flops 5000000000 | bytes 16777216 | tf_op jit(solution)/shard_map/expert_rows/pallas_call | solution.py:829
  215.8 83.0 %exchange_2.1.back_ref = bf16[32,48,512]{2,1,0:T(8,128)(2,1)} custom-call(bf16[32,48,512]{2,1,0:T(8,128)(2,1)} %expert_rows.1.src_ref), custom_call_target="tpu_custom_call" | custom-call | flops 1000000 | bytes 209715200 | tf_op jit(solution)/shard_map/exchange_2/pallas_call | solution.py:764
  298.9 4.0 %combine.1 = bf16[128,2048]{1,0:T(8,128)(2,1)} custom-call(bf16[128,2048]{1,0:T(8,128)(2,1)} %residual_ref.3, bf16[2,128,1024]{2,1,0:T(8,128)(2,1)} %swap.1.proj_ref, s32[128,2]{1,0:T(8,128)} %copy.22.index_ref, f32[128,2]{1,0:T(8,128)} %copy.23.weight_ref, bf16[32,48,512]{2,1,0:T(8,128)(2,1)} %exchange_2.1.back_ref), custom_call_target="tpu_custom_call" | custom-call | flops 1000000000 | bytes 8388608 | tf_op jit(solution)/shard_map/combine/pallas_call | solution.py:879
Async XLA Ops:
  6.5 1.6 copy-start
  6.6 87.1 %all-gather.5.cloned.1.call-start = ((), (), s32[]{:S(2)}) async-start(), calls=%async_computation | async-start | bytes 5242880 | tf_op jit(solution)/shard_map/all_gather | solution.py:902
  9.4 194.9 %all-gather.7.cloned.1.call-start = ((), (), s32[]{:S(2)}) async-start(), calls=%async_computation.1 | async-start | bytes 5242880 | tf_op jit(solution)/shard_map/all_gather | solution.py:910
  27.9 41.0 %copy-start.1 = (s32[128,2]{0,1:T(2,128)S(1)}, s32[128,2]{0,1:T(2,128)}, u32[]{:S(2)}) copy-start(s32[128,2]{0,1:T(2,128)} %param.33) | copy-start | bytes 3076
  27.9 41.8 %copy-start.2 = (f32[128,2]{0,1:T(2,128)S(1)}, f32[128,2]{0,1:T(2,128)}, u32[]{:S(2)}) copy-start(f32[128,2]{0,1:T(2,128)} %param.34) | copy-start | bytes 3076
Sparse Core Ops, SparseCore 0:
  9.5 68.6 all-gather.4
  80.0 69.0 all-gather.6

commit v3 on v2

--- a/solution.py
+++ b/solution.py
@@ -388,19 +388,30 @@
     enter_ref, out_ref,
 ):
     ones = head_ones()
-    for p in range(pairs):
-        cols = slice(p * LANES, (p + 1) * LANES)
-        state = stacked(enter_ref[p])
-        for start in range(0, length, 128):
-            rows = slice(start, start + 128)
-            value = value_ref[rows, cols].astype(f32)
-            own = recept_ref[rows, cols].astype(f32) * key_ref[rows, cols].astype(f32) * self_ref[:, cols]
-            own = dot_split_left(own, ones) * value
-            read = dot(map_ref[rows, cols], state) + own_ref[rows, cols]
-            center = read - dot_split_left(read, ones) * (1.0 / HEAD)
-            spread = dot_split_left(center * center, ones) * (1.0 / HEAD)
-            normed = center * lax.rsqrt(spread + GROUP_EPS) * gain_ref[:, cols]
-            out_ref[rows, cols] = ((normed + own) * gate_ref[rows, cols].astype(f32)).astype(bf16)
+    step = 128
+
+    def some(i, _):
+        rows = pl.ds(pl.multiple_of(i * step, step), step)
+        every = [slice(p * LANES, (p + 1) * LANES) for p in range(pairs)]
+        own = [
+            recept_ref[rows, c].astype(f32) * key_ref[rows, c].astype(f32) * self_ref[:, c] for c in every
+        ]
+        read = [
+            dot(map_ref[rows, c], stacked(enter_ref[p])) + own_ref[rows, c] for p, c in enumerate(every)
+        ]
+        own = [dot_split_left(x, ones) for x in own]
+        mean = [dot_split_left(x, ones) * (1.0 / HEAD) for x in read]
+        center = [x - y for x, y in zip(read, mean)]
+        spread = [dot_split_left(x * x, ones) * (1.0 / HEAD) for x in center]
+        for p, c in enumerate(every):
+            normed = center[p] * lax.rsqrt(spread[p] + GROUP_EPS) * gain_ref[:, c]
+            value = value_ref[rows, c].astype(f32)
+            out_ref[rows, c] = (
+                (normed + own[p] * value) * gate_ref[rows, c].astype(f32)
+            ).astype(bf16)
+        return 0
+
+    lax.fori_loop(0, length // step, some, 0)
 
 
 def readout(recept, key, value, gate, gain, self_weight, maps, own, enter):
@@ -469,52 +480,6 @@
     )(residual, proj, gain, index)
 
 
-def exchange_kernel(n, src_ref, out_ref, own_sem, sent, came):
-    me = lax.axis_index("sp")
-    barrier = pltpu.get_barrier_semaphore()
-
-    def greet(k, _):
-        pl.semaphore_signal(
-            barrier, inc=1, device_id={"sp": lax.rem(me + k, n)}, device_id_type=MESH
-        )
-        return 0
-
-    lax.fori_loop(1, n, greet, 0)
-    own = pltpu.make_async_copy(src_ref.at[me], out_ref.at[me], own_sem)
-    own.start()
-    pl.semaphore_wait(barrier, n - 1)
-
-    def copy(k):
-        to = lax.rem(me + k, n)
-        return pltpu.make_async_remote_copy(
-            src_ref=src_ref.at[to], dst_ref=out_ref.at[me], send_sem=sent.at[k], recv_sem=came.at[k],
-            device_id={"sp": to}, device_id_type=MESH,
-        )
-
-    def start(k, _):
-        away = n // 2 - lax.div(k, 2)
-        copy(jnp.where(lax.rem(k, 2) == 0, away, n - away)).start()
-        return 0
-
-    def arrived(k):
-        frm = lax.rem(me + n - k, n)
-        return pltpu.make_async_remote_copy(
-            src_ref=src_ref.at[frm], dst_ref=out_ref.at[frm], send_sem=sent.at[k], recv_sem=came.at[k],
-            device_id={"sp": frm}, device_id_type=MESH,
-        )
-
-    copy(n // 2).start()
-    lax.fori_loop(2, n, start, 0)
-    own.wait()
-
-    def finish(k, _):
-        arrived(k).wait_recv()
-        copy(k).wait_send()
-        return 0
-
-    lax.fori_loop(1, n, finish, 0)
-
-
 def other_core(me):
     return me + 1 - 2 * lax.rem(me, 2)
 
@@ -760,23 +725,6 @@
     )(blocks, first, second)
 
 
-def exchange(blocks, n, number):
-    return pl.pallas_call(
-        functools.partial(exchange_kernel, n),
-        name=f"exchange_{number}",
-        out_shape=jax.ShapeDtypeStruct(blocks.shape, blocks.dtype),
-        in_specs=[VMEM_SPEC],
-        out_specs=VMEM_SPEC,
-        scratch_shapes=[
-            pltpu.SemaphoreType.DMA,
-            pltpu.SemaphoreType.DMA((n,)),
-            pltpu.SemaphoreType.DMA((n,)),
-        ],
-        compiler_params=pltpu.CompilerParams(collective_id=number, has_side_effects=True),
-        cost_estimate=pl.CostEstimate(flops=10**6, bytes_accessed=200 << 20, transcendentals=0),
-    )(blocks)
-
-
 def reorder(capacity, to_rows):
     many = BLOCK * QUARTERS * capacity
     square = (many, many)
@@ -786,64 +734,125 @@
     return jnp.where(out == place, 1.0, 0.0).astype(bf16)
 
 
-def expert_kernel(n, capacity, came_ref, gate_ref, up_ref, down_ref, out_ref, rows_ref, total_ref):
-    j = pl.program_id(0)
+def expert_kernel(
+    n, capacity, came_ref, gate_ref, up_ref, down_ref, out_ref,
+    gates, ups, downs, rows_ref, back_ref, load_sem, sent, came,
+):
+    me = lax.axis_index("sp")
     block = QUARTERS * capacity
     height = BLOCK * capacity
-    part = rows_ref.shape[1] // QUARTERS
-
-    @pl.when(j == 0)
-    def _():
-        order = reorder(capacity, True)
-        for g in range(n // BLOCK):
+    part = out_ref.shape[2]
+    pieces = gates.shape[0]
+    groups = n // BLOCK
+    loads = []
+    for j in range(pieces):
+        for w, (source, target) in enumerate(((gate_ref, gates), (up_ref, ups), (down_ref, downs))):
+            loads.append(pltpu.make_async_copy(source.at[j], target.at[j], load_sem.at[j, w]))
+    for load in loads:
+        load.start()
+    barrier = pltpu.get_barrier_semaphore()
+
+    def greet(k, _):
+        pl.semaphore_signal(
+            barrier, inc=1, device_id={"sp": lax.rem(me + k, n)}, device_id_type=MESH
+        )
+        return 0
+
+    lax.fori_loop(1, n, greet, 0)
+    gather_order, spread_order = reorder(capacity, True), reorder(capacity, False)
+    for load in loads:
+        load.wait()
+    pl.semaphore_wait(barrier, n - 1)
+
+    def home(device):
+        return pltpu.make_async_remote_copy(
+            src_ref=back_ref.at[device], dst_ref=out_ref.at[me], send_sem=sent.at[device],
+            recv_sem=came.at[me], device_id={"sp": device}, device_id_type=MESH,
+        )
+
+    def work(c, _):
+        own_group = lax.div(me, BLOCK)
+        both = (
+            lax.rem(own_group + groups // 2 + c, groups),
+            lax.rem(own_group + groups // 2 - 1 - c + groups, groups),
+        )
+        for i, g in enumerate(both):
             lines = jnp.concatenate([came_ref[g * BLOCK + k] for k in range(BLOCK)], axis=0)
-            moved = dot(order, lines).astype(bf16)
+            moved = dot(gather_order, lines).astype(bf16)
             for q in range(QUARTERS):
-                rows_ref[g * height : (g + 1) * height, q * part : (q + 1) * part] = moved[
+                rows_ref[i * height : (i + 1) * height, q * part : (q + 1) * part] = moved[
                     q * height : (q + 1) * height
                 ]
-        total_ref[...] = jnp.zeros_like(total_ref)
-
-    gated = dot(rows_ref[...], gate_ref[0])
-    upward = dot(rows_ref[...], up_ref[0])
-    hidden = (gated * sigmoid(gated) * upward).astype(bf16)
-    total_ref[...] += dot(hidden, down_ref[0])
-
-    @pl.when(j == pl.num_programs(0) - 1)
-    def _():
-        order = reorder(capacity, False)
-        for g in range(n // BLOCK):
-            rows = slice(g * height, (g + 1) * height)
+        rows = rows_ref[...]
+        hidden = []
+        for j in range(pieces):
+            gated = dot(rows, gates[j])
+            hidden.append((gated * sigmoid(gated) * dot(rows, ups[j])).astype(bf16))
+        total = dot(hidden[0], downs[0])
+        for j in range(1, pieces):
+            total = total + dot(hidden[j], downs[j])
+        total = total.astype(bf16)
+        for i, g in enumerate(both):
             lines = jnp.concatenate(
-                [total_ref[rows, q * part : (q + 1) * part] for q in range(QUARTERS)], axis=0
+                [total[i * height : (i + 1) * height, q * part : (q + 1) * part] for q in range(QUARTERS)],
+                axis=0,
             )
-            moved = dot(order, lines).astype(bf16)
+            moved = dot(spread_order, lines).astype(bf16)
             for k in range(BLOCK):
-                out_ref[g * BLOCK + k] = moved[k * block : (k + 1) * block]
-
-
-def expert_rows(came, gate, up, down, capacity):
+                device = g * BLOCK + k
+                result = moved[k * block : (k + 1) * block]
+                back_ref[device] = result
+
+                @pl.when(device == me)
+                def _():
+                    out_ref[me] = result
+
+        for g in both:
+            for k in range(BLOCK):
+                device = g * BLOCK + k
+
+                @pl.when(device != me)
+                def _():
+                    home(device).start()
+
+        return 0
+
+    lax.fori_loop(0, groups // 2, work, 0)
+
+    def finish(k, _):
+        frm = lax.rem(me + k, n)
+        pltpu.make_async_remote_copy(
+            src_ref=back_ref.at[frm], dst_ref=out_ref.at[frm], send_sem=sent.at[frm],
+            recv_sem=came.at[frm], device_id={"sp": frm}, device_id_type=MESH,
+        ).wait_recv()
+        home(frm).wait_send()
+        return 0
+
+    lax.fori_loop(1, n, finish, 0)
+
+
+def expert_rows(came, gate, up, down, capacity, number):
     n, block, part = came.shape
     pieces, width, units = gate.shape
-    whole = pl.BlockSpec((n, block, part), lambda j: (0, 0, 0))
+    any_spec = pl.BlockSpec(memory_space=pl.ANY)
     return pl.pallas_call(
         functools.partial(expert_kernel, n, capacity),
         name="expert_rows",
-        grid=(pieces,),
         out_shape=jax.ShapeDtypeStruct(came.shape, bf16),
-        in_specs=[
-            whole,
-            pl.BlockSpec((1, width, units), lambda j: (j, 0, 0)),
-            pl.BlockSpec((1, width, units), lambda j: (j, 0, 0)),
-            pl.BlockSpec((1, units, width), lambda j: (j, 0, 0)),
+        in_specs=[VMEM_SPEC, any_spec, any_spec, any_spec],
+        out_specs=VMEM_SPEC,
+        scratch_shapes=[
+            pltpu.VMEM(gate.shape, bf16),
+            pltpu.VMEM(up.shape, bf16),
+            pltpu.VMEM(down.shape, bf16),
+            pltpu.VMEM((2 * BLOCK * capacity, width), bf16),
+            pltpu.VMEM(came.shape, bf16),
+            pltpu.SemaphoreType.DMA((pieces, 3)),
+            pltpu.SemaphoreType.DMA((n,)),
+            pltpu.SemaphoreType.DMA((n,)),
         ],
-        out_specs=whole,
-        scratch_shapes=[
-            pltpu.VMEM((n * capacity, width), bf16),
-            pltpu.VMEM((n * capacity, width), f32),
-        ],
-        compiler_params=pltpu.CompilerParams(dimension_semantics=("arbitrary",)),
-        cost_estimate=pl.CostEstimate(flops=5 * 10**9, bytes_accessed=16 << 20, transcendentals=0),
+        compiler_params=pltpu.CompilerParams(collective_id=number, has_side_effects=True),
+        cost_estimate=pl.CostEstimate(flops=5 * 10**9, bytes_accessed=200 << 20, transcendentals=0),
     )(came, gate, up, down)
 
 
@@ -924,8 +933,7 @@
     came, gate, up = exchange_and_gather(
         outgoing, gate_weight_experts[0], up_weight_experts[0], n, lax.axis_size("tp"), 1
     )
-    results = expert_rows(came, gate, up, down, capacity)
-    back = exchange(results, n, 2)
+    back = expert_rows(came, gate, up, down, capacity, 2)
     return combine(residual, proj, routed_expert_index, routed_expert_weight, back, capacity)
 
 

time: 310 us -> 302 us (0.974)
  Pallas kernels: 285 us -> 277 us
    pallas_call x1 -> x0, Pallas kernels: 83 us -> none  [exchange(): pl.pallas_call(functools.partial(exchange_kernel, n), name=f'exchange_{nu...]
    pallas_call x1, Pallas kernels: 11.5 us -> 86.5 us  [expert_rows(): pl.pallas_call(functools.partial(expert_kernel, n, capacity), name='exper...]
  transfers between devices with their start and end apart: 2 -> 2, of which waited for: 0 -> 0; matrix products, arithmetic and copies ran while one was open for 3% -> 3% of each run, Pallas kernels for 60% -> 62%
where the time goes in v3:
time: 302 us
  Pallas kernels  277 us (92%)
  between operations  13.5 us (4%)
  local copies, waits for them, and re-layouts  5.78 us (2%)
  matrix products  4.56 us (2%)
    pallas_call x1, Pallas kernels, exchange_and_gather(): pl.pallas_call(functools.partial(exchange_gather_kernel, n, m), name=f'ex...  102 us
    pallas_call x1, Pallas kernels, expert_rows(): pl.pallas_call(functools.partial(expert_kernel, n, capacity), name='exper...  86.5 us
    pallas_call x1, Pallas kernels, prefix_states(): pl.pallas_call(functools.partial(prefix_kernel, n, pairs), name='prefix_s...  40.9 us
    pallas_call x1, Pallas kernels, mixer_local(): pl.pallas_call(functools.partial(mixer_kernel, pairs, chunks), name='mixe...  16.9 us
    pallas_call x1, Pallas kernels, spread(): pl.pallas_call(functools.partial(spread_kernel, m), name='spread', out_sh...  15.2 us
  transfers between devices with their start and end apart: 2, of which 0 were waited for; matrix products, arithmetic and copies ran while one was open for 3% of the time, Pallas kernels for 62%

profile of v3, /device:TPU:33, one launch (start us, length us, event | category | flops | bytes accessed | tf_op | source)
XLA Modules:
  0.0 301.5 jit_solution(14004406050580874468)
XLA Ops:
  6.5 0.0 copy-start
  6.6 0.0 all-gather.5.cloned.1.call-start
  6.6 1.6 copy-done
  8.1 1.2 constant_dynamic-slice_fusion
  9.3 0.1 all-gather.5.cloned.1.call-update
  9.4 0.1 all-gather.7.cloned.1.call-start
  9.4 1.6 copy.20.offset_ref
  11.0 16.9 %mixer_local.1 = (bf16[4,2,64,128]{3,2,1,0:T(8,128)(2,1)}, bf16[512,512]{1,0:T(8,128)(2,1)}, f32[512,512]{1,0:T(8,128)}) custom-call(bf16[512,512]{1,0:T(8,128)(2,1)} %recept_ref.3, bf16[512,512]{1,0:T(8,128)(2,1)} %key_ref.3, bf16[512,512]{1,0:T(8,128)(2,1)} %value_ref.3, bf16[512,512]{1,0:T(8,128)(2,1)} %decay_ref.1, bf16[512,512]{1,0:T(8,128)(2,1)} %rate_ref.1, ...), custom_call_target="tpu_custom_call" | custom-call | flops 5368709120 | bytes 3145728 | tf_op jit(solution)/shard_map/mixer_local/pallas_call | solution.py:241
  27.9 0.0 copy-start.1
  27.9 0.0 copy-start.2
  27.9 40.9 %prefix_states.1.enter_ref = bf16[4,64,128]{2,1,0:T(8,128)(2,1)} custom-call(bf16[4,2,64,128]{3,2,1,0:T(8,128)(2,1)} %get-tuple-element.15.summary_ref), custom_call_target="tpu_custom_call" | custom-call | flops 1000000000 | bytes 62914560 | tf_op jit(solution)/shard_map/prefix_states/pallas_call | solution.py:366
  68.8 0.1 all-gather.7.cloned.1.call-update
  68.9 0.0 copy-done.1
  68.9 0.7 copy.22.index_ref
  69.6 0.0 copy-done.2
  69.6 0.7 copy.23.weight_ref
  70.4 5.1 %readout.1 = bf16[512,512]{1,0:T(8,128)(2,1)} custom-call(bf16[512,512]{1,0:T(8,128)(2,1)} %recept_ref.3, bf16[512,512]{1,0:T(8,128)(2,1)} %key_ref.3, bf16[512,512]{1,0:T(8,128)(2,1)} %value_ref.3, bf16[512,512]{1,0:T(8,128)(2,1)} %gate_ref.1, f32[1,512]{1,0:T(1,128)} %bitcast.24, f32[1,512]{1,0:T(1,128)} %bitcast.25, ...), custom_call_target="tpu_custom_call" | custom-call | flops 1000000000 | bytes 16777216 | tf_op jit(solution)/shard_map/readout/pallas_call | solution.py:419
  75.4 15.2 %spread.1 = bf16[2,4,128,512]{3,2,1,0:T(8,128)(2,1)} custom-call(bf16[4,128,512]{2,1,0:T(8,128)(2,1)} %bitcast.20), custom_call_target="tpu_custom_call" | custom-call | flops 1000000 | bytes 41943040 | tf_op jit(solution)/shard_map/spread/pallas_call | solution.py:545
  90.7 0.0 all-gather.5.cloned.1.call-done
  90.7 4.6 %fusion.src_ref = bf16[2,128,1024]{2,1,0:T(8,128)(2,1)} fusion(bf16[2,4,128,512]{3,2,1,0:T(8,128)(2,1)} %spread.1, bf16[4,512,1024,1]{2,1,0,3:T(8,128)(2,1)} %bitcast.26), kind=kOutput, calls=%fused_computation.1 | convolution fusion | flops 1074003968 | bytes 5767168 | tf_op jit(solution)/shard_map/hjrc,jcd->hrd/dot_general | solution.py:926
  95.3 3.5 %swap.1.proj_ref = bf16[2,128,1024]{2,1,0:T(8,128)(2,1)} custom-call(bf16[2,128,1024]{2,1,0:T(8,128)(2,1)} %fusion.src_ref), custom_call_target="tpu_custom_call" | custom-call | flops 1000000 | bytes 4194304 | tf_op jit(solution)/shard_map/swap/pallas_call | solution.py:579
  98.7 3.9 %build.1.src_ref = bf16[32,48,512]{2,1,0:T(8,128)(2,1)} custom-call(bf16[128,2048]{1,0:T(8,128)(2,1)} %residual_ref.3, bf16[2,128,1024]{2,1,0:T(8,128)(2,1)} %swap.1.proj_ref, f32[1,2048]{1,0:T(1,128)} %bitcast.28, s32[128,2]{1,0:T(8,128)} %copy.22.index_ref), custom_call_target="tpu_custom_call" | custom-call | flops 1000000000 | bytes 8388608 | tf_op jit(solution)/shard_map/build/pallas_call | solution.py:472
  102.6 101.5 %exchange_1.1 = (bf16[32,48,512]{2,1,0:T(8,128)(2,1)}, bf16[4,2048,256]{2,1,0:T(8,128)(2,1)}, bf16[4,2048,256]{2,1,0:T(8,128)(2,1)}) custom-call(bf16[32,48,512]{2,1,0:T(8,128)(2,1)} %build.1.src_ref, bf16[2048,256]{1,0:T(8,128)(2,1)} %bitcast.21, bf16[2048,256]{1,0:T(8,128)(2,1)} %bitcast.22), custom_call_target="tpu_custom_call" | custom-call | flops 1000000 | bytes 209715200 | tf_op jit(solution)/shard_map/exchange_1/pallas_call | solution.py:705
  204.2 0.0 all-gather.7.cloned.1.call-done
  204.2 86.5 %expert_rows.1.back_ref = bf16[32,48,512]{2,1,0:T(8,128)(2,1)} custom-call(bf16[32,48,512]{2,1,0:T(8,128)(2,1)} %get-tuple-element.17.came_ref, bf16[4,2048,256]{2,1,0:T(8,128)(2,1)} %get-tuple-element.18.gate_ref, bf16[4,2048,256]{2,1,0:T(8,128)(2,1)} %get-tuple-element.19.up_ref, bf16[4,256,2048]{2,1,0:T(8,128)(2,1)} %bitcast.27), custom_call_target="tpu_custom_call" | custom-call | flops 5000000000 | bytes 209715200 | tf_op jit(solution)/shard_map/expert_rows/pallas_call | solution.py:838
  290.7 4.0 %combine.1 = bf16[128,2048]{1,0:T(8,128)(2,1)} custom-call(bf16[128,2048]{1,0:T(8,128)(2,1)} %residual_ref.3, bf16[2,128,1024]{2,1,0:T(8,128)(2,1)} %swap.1.proj_ref, s32[128,2]{1,0:T(8,128)} %copy.22.index_ref, f32[128,2]{1,0:T(8,128)} %copy.23.weight_ref, bf16[32,48,512]{2,1,0:T(8,128)(2,1)} %expert_rows.1.back_ref), custom_call_target="tpu_custom_call" | custom-call | flops 1000000000 | bytes 8388608 | tf_op jit(solution)/shard_map/combine/pallas_call | solution.py:888
Async XLA Ops:
  6.5 1.6 copy-start
  6.6 84.1 %all-gather.5.cloned.1.call-start = ((), (), s32[]{:S(2)}) async-start(), calls=%async_computation | async-start | bytes 5242880 | tf_op jit(solution)/shard_map/all_gather | solution.py:911
  9.4 194.8 %all-gather.7.cloned.1.call-start = ((), (), s32[]{:S(2)}) async-start(), calls=%async_computation.1 | async-start | bytes 5242880 | tf_op jit(solution)/shard_map/all_gather | solution.py:919
  27.9 41.0 %copy-start.1 = (s32[128,2]{0,1:T(2,128)S(1)}, s32[128,2]{0,1:T(2,128)}, u32[]{:S(2)}) copy-start(s32[128,2]{0,1:T(2,128)} %param.33) | copy-start | bytes 3076
  27.9 41.7 %copy-start.2 = (f32[128,2]{0,1:T(2,128)S(1)}, f32[128,2]{0,1:T(2,128)}, u32[]{:S(2)}) copy-start(f32[128,2]{0,1:T(2,128)} %param.34) | copy-start | bytes 3076
Sparse Core Ops, SparseCore 0:
  9.5 68.6 all-gather.4
  80.0 71.8 all-gather.6

commit v4 on v3

--- a/solution.py
+++ b/solution.py
@@ -264,8 +264,52 @@
     )(recept, key, value, decay, rate, offset, decay_bias, rate_bias)
 
 
-def prefix_kernel(n, pairs, summary_ref, enter_ref, got, states, entry, sent1, came1, sent2, came2):
-    me = lax.axis_index("sp")
+def prefix_kernel(
+    n, m, pairs, summary_ref, shard_ref, enter_ref, whole_ref,
+    got, states, entry, stage, sent1, came1, sent2, came2,
+    in_sem, out_sem, ring_sent, ring_came, pass_sent, pass_came,
+):
+    me, col = lax.axis_index("sp"), lax.axis_index("tp")
+    right, left = lax.rem(col + 1, m), lax.rem(col + m - 1, m)
+    half = stage.shape[0] // 2
+    load = pltpu.make_async_copy(shard_ref.at[pl.ds(0, 2 * half)], stage, in_sem)
+    store = pltpu.make_async_copy(stage, whole_ref.at[col], out_sem)
+    load.start()
+
+    def part(h):
+        return pl.ds(h * half, half)
+
+    def hop(d, h):
+        return pltpu.make_async_remote_copy(
+            src_ref=stage.at[part(h)], dst_ref=whole_ref.at[col, part(h)],
+            send_sem=ring_sent.at[d, h], recv_sem=ring_came.at[d, h],
+            device_id={"tp": (right, left)[d]}, device_id_type=MESH,
+        )
+
+    def hop_in(d, h):
+        frm = (left, right)[d]
+        return pltpu.make_async_remote_copy(
+            src_ref=stage.at[part(h)], dst_ref=whole_ref.at[frm, part(h)],
+            send_sem=ring_sent.at[d, h], recv_sem=ring_came.at[d, h],
+            device_id={"tp": frm}, device_id_type=MESH,
+        )
+
+    def onward(d):
+        frm = (left, right)[d]
+        return pltpu.make_async_remote_copy(
+            src_ref=whole_ref.at[frm, part(d)], dst_ref=whole_ref.at[frm, part(d)],
+            send_sem=pass_sent.at[d], recv_sem=pass_came.at[d],
+            device_id={"tp": (right, left)[d]}, device_id_type=MESH,
+        )
+
+    def onward_in(d):
+        frm = lax.rem(col + 2, m)
+        return pltpu.make_async_remote_copy(
+            src_ref=whole_ref.at[frm, part(d)], dst_ref=whole_ref.at[frm, part(d)],
+            send_sem=pass_sent.at[d], recv_sem=pass_came.at[d],
+            device_id={"tp": (left, right)[d]}, device_id_type=MESH,
+        )
+
     stride = n // pairs
     works = lax.rem(me, stride) == 0
     mine = lax.div(me, stride)
@@ -273,6 +317,9 @@
 
     def greet(device):
         pl.semaphore_signal(barrier, inc=1, device_id={"sp": device}, device_id_type=MESH)
+
+    for side in (left, right):
+        pl.semaphore_signal(barrier, inc=1, device_id={"tp": side}, device_id_type=MESH)
 
     @pl.when(works)
     def _():
@@ -281,13 +328,13 @@
             return 0
 
         lax.fori_loop(1, n, body, 0)
-        pl.semaphore_wait(barrier, n - 1)
+        pl.semaphore_wait(barrier, n + 1)
 
     @pl.when(jnp.logical_not(works))
     def _():
         for p in range(pairs):
             greet(p * stride)
-        pl.semaphore_wait(barrier, pairs)
+        pl.semaphore_wait(barrier, pairs + 2)
 
     def outward(p):
         return pltpu.make_async_remote_copy(
@@ -316,6 +363,11 @@
         def _():
             got[me] = summary_ref[p]
 
+    load.wait()
+    for d, h in ((0, 0), (1, 1), (0, 1), (1, 0)):
+        hop(d, h).start()
+    store.start()
+
     @pl.when(works)
     def _():
         def step(i, state):
@@ -336,6 +388,10 @@
             return state + (moved + added)
 
         lax.fori_loop(0, n, step, jnp.zeros((HEAD, LANES), f32))
+
+    for d in range(2):
+        hop_in(d, d).wait_recv()
+        onward(d).start()
 
     for p in range(pairs):
         @pl.when(me != p * stride)
@@ -360,27 +416,46 @@
 
         lax.fori_loop(0, n, body, 0)
 
-
-def prefix_states(summary, n):
+    store.wait()
+    for d in range(2):
+        hop_in(d, 1 - d).wait_recv()
+        onward_in(d).wait_recv()
+        onward(d).wait_send()
+        for h in range(2):
+            hop(d, h).wait_send()
+
+
+def prefix_states(summary, shard, early, n, m):
     pairs = summary.shape[0]
+    any_spec = pl.BlockSpec(memory_space=pl.ANY)
     return pl.pallas_call(
-        functools.partial(prefix_kernel, n, pairs),
+        functools.partial(prefix_kernel, n, m, pairs),
         name="prefix_states",
-        out_shape=jax.ShapeDtypeStruct((pairs, HEAD, LANES), bf16),
-        in_specs=[VMEM_SPEC],
-        out_specs=VMEM_SPEC,
+        out_shape=(
+            jax.ShapeDtypeStruct((pairs, HEAD, LANES), bf16),
+            jax.ShapeDtypeStruct((m, early, shard.shape[1]), shard.dtype),
+        ),
+        in_specs=[VMEM_SPEC, any_spec],
+        out_specs=(VMEM_SPEC, any_spec),
         scratch_shapes=[
             pltpu.VMEM((n, 2, HEAD, LANES), bf16),
             pltpu.VMEM((n, HEAD, LANES), bf16),
             pltpu.VMEM((pairs, HEAD, LANES), bf16),
+            pltpu.VMEM((early, shard.shape[1]), shard.dtype),
             pltpu.SemaphoreType.DMA((pairs,)),
             pltpu.SemaphoreType.DMA((n,)),
             pltpu.SemaphoreType.DMA((n,)),
             pltpu.SemaphoreType.DMA((pairs,)),
+            pltpu.SemaphoreType.DMA,
+            pltpu.SemaphoreType.DMA,
+            pltpu.SemaphoreType.DMA((2, 2)),
+            pltpu.SemaphoreType.DMA((2, 2)),
+            pltpu.SemaphoreType.DMA((2,)),
+            pltpu.SemaphoreType.DMA((2,)),
         ],
         compiler_params=pltpu.CompilerParams(collective_id=0, has_side_effects=True),
         cost_estimate=pl.CostEstimate(flops=10**9, bytes_accessed=60 << 20, transcendentals=0),
-    )(summary)
+    )(summary, shard)
 
 
 def readout_kernel(
@@ -588,11 +663,13 @@
     )(blocks)
 
 
-def exchange_gather_kernel(n, m, src_ref, first_ref, second_ref, out_ref, first_all, second_all,
-                           stage, own_sem, sent, came, in_sem, out_sem, ring_sent, ring_came, pass_sent, pass_came):
+def exchange_gather_kernel(n, m, skip, src_ref, first_ref, second_ref, out_ref, first_all, second_all,
+                           first_stage, second_stage, own_sem, sent, came, in_sem, out_sem, ring_sent, ring_came, pass_sent, pass_came):
     me, col = lax.axis_index("sp"), lax.axis_index("tp")
     right, left = lax.rem(col + 1, m), lax.rem(col + m - 1, m)
-    shards, wholes = (first_ref, second_ref), (first_all, second_all)
+    counts = (first_ref.shape[0] - skip, second_ref.shape[0])
+    shards = (first_ref.at[pl.ds(skip, counts[0])], second_ref)
+    wholes, stage = (first_all, second_all), (first_stage, second_stage)
     barrier = pltpu.get_barrier_semaphore()
 
     def greet(k, _):
@@ -606,8 +683,8 @@
     lax.fori_loop(1, n, greet, 0)
     own = pltpu.make_async_copy(src_ref.at[me], out_ref.at[me], own_sem)
     own.start()
-    loads = [pltpu.make_async_copy(shards[a], stage.at[a], in_sem.at[a]) for a in range(2)]
-    stores = [pltpu.make_async_copy(stage.at[a], wholes[a].at[col], out_sem.at[a]) for a in range(2)]
+    loads = [pltpu.make_async_copy(shards[a], stage[a], in_sem.at[a]) for a in range(2)]
+    stores = [pltpu.make_async_copy(stage[a], wholes[a].at[col], out_sem.at[a]) for a in range(2)]
     for load in loads:
         load.start()
     for load in loads:
@@ -633,14 +710,12 @@
             device_id={"sp": frm}, device_id_type=MESH,
         )
 
-    half = first_ref.shape[0] // 2
-
-    def rows(h):
-        return pl.ds(h * half, half)
+    def rows(a, h):
+        return pl.ds(h * (counts[a] // 2), counts[a] // 2)
 
     def hop(a, d, h):
         return pltpu.make_async_remote_copy(
-            src_ref=stage.at[a, rows(h)], dst_ref=wholes[a].at[col, rows(h)],
+            src_ref=stage[a].at[rows(a, h)], dst_ref=wholes[a].at[col, rows(a, h)],
             send_sem=ring_sent.at[a, d, h], recv_sem=ring_came.at[a, d, h],
             device_id={"tp": (right, left)[d]}, device_id_type=MESH,
         )
@@ -648,7 +723,7 @@
     def hop_in(a, d, h):
         frm = (left, right)[d]
         return pltpu.make_async_remote_copy(
-            src_ref=stage.at[a, rows(h)], dst_ref=wholes[a].at[frm, rows(h)],
+            src_ref=stage[a].at[rows(a, h)], dst_ref=wholes[a].at[frm, rows(a, h)],
             send_sem=ring_sent.at[a, d, h], recv_sem=ring_came.at[a, d, h],
             device_id={"tp": frm}, device_id_type=MESH,
         )
@@ -656,7 +731,7 @@
     def onward(a, d):
         frm = (left, right)[d]
         return pltpu.make_async_remote_copy(
-            src_ref=wholes[a].at[frm, rows(d)], dst_ref=wholes[a].at[frm, rows(d)],
+            src_ref=wholes[a].at[frm, rows(a, d)], dst_ref=wholes[a].at[frm, rows(a, d)],
             send_sem=pass_sent.at[a, d], recv_sem=pass_came.at[a, d],
             device_id={"tp": (right, left)[d]}, device_id_type=MESH,
         )
@@ -664,7 +739,7 @@
     def onward_in(a, d):
         frm = lax.rem(col + 2, m)
         return pltpu.make_async_remote_copy(
-            src_ref=wholes[a].at[frm, rows(d)], dst_ref=wholes[a].at[frm, rows(d)],
+            src_ref=wholes[a].at[frm, rows(a, d)], dst_ref=wholes[a].at[frm, rows(a, d)],
             send_sem=pass_sent.at[a, d], recv_sem=pass_came.at[a, d],
             device_id={"tp": (left, right)[d]}, device_id_type=MESH,
         )
@@ -699,17 +774,22 @@
                 hop(a, d, h).wait_send()
 
 
-def exchange_and_gather(blocks, first, second, n, m, number):
+def exchange_and_gather(blocks, first, second, skip, n, m, number):
     any_spec = pl.BlockSpec(memory_space=pl.ANY)
-    whole = jax.ShapeDtypeStruct((m,) + first.shape, first.dtype)
+    tail = (first.shape[0] - skip, first.shape[1])
     return pl.pallas_call(
-        functools.partial(exchange_gather_kernel, n, m),
+        functools.partial(exchange_gather_kernel, n, m, skip),
         name=f"exchange_{number}",
-        out_shape=(jax.ShapeDtypeStruct(blocks.shape, blocks.dtype), whole, whole),
+        out_shape=(
+            jax.ShapeDtypeStruct(blocks.shape, blocks.dtype),
+            jax.ShapeDtypeStruct((m,) + tail, first.dtype),
+            jax.ShapeDtypeStruct((m,) + second.shape, second.dtype),
+        ),
         in_specs=[VMEM_SPEC, any_spec, any_spec],
         out_specs=(VMEM_SPEC, any_spec, any_spec),
         scratch_shapes=[
-            pltpu.VMEM((2,) + first.shape, first.dtype),
+            pltpu.VMEM(tail, first.dtype),
+            pltpu.VMEM(second.shape, second.dtype),
             pltpu.SemaphoreType.DMA,
             pltpu.SemaphoreType.DMA((n,)),
             pltpu.SemaphoreType.DMA((n,)),
@@ -735,7 +815,7 @@
 
 
 def expert_kernel(
-    n, capacity, came_ref, gate_ref, up_ref, down_ref, out_ref,
+    n, capacity, came_ref, early_ref, gate_ref, up_ref, down_ref, out_ref,
     gates, ups, downs, rows_ref, back_ref, load_sem, sent, came,
 ):
     me = lax.axis_index("sp")
@@ -746,8 +826,15 @@
     groups = n // BLOCK
     loads = []
     for j in range(pieces):
-        for w, (source, target) in enumerate(((gate_ref, gates), (up_ref, ups), (down_ref, downs))):
-            loads.append(pltpu.make_async_copy(source.at[j], target.at[j], load_sem.at[j, w]))
+        early = early_ref.shape[1]
+        moves = (
+            (early_ref.at[j], gates.at[j, pl.ds(0, early)]),
+            (gate_ref.at[j], gates.at[j, pl.ds(early, gate_ref.shape[1])]),
+            (up_ref.at[j], ups.at[j]),
+            (down_ref.at[j], downs.at[j]),
+        )
+        for w, (source, target) in enumerate(moves):
+            loads.append(pltpu.make_async_copy(source, target, load_sem.at[j, w]))
     for load in loads:
         load.start()
     barrier = pltpu.get_barrier_semaphore()
@@ -831,29 +918,29 @@
     lax.fori_loop(1, n, finish, 0)
 
 
-def expert_rows(came, gate, up, down, capacity, number):
+def expert_rows(came, early, gate, up, down, capacity, number):
     n, block, part = came.shape
-    pieces, width, units = gate.shape
+    pieces, width, units = up.shape
     any_spec = pl.BlockSpec(memory_space=pl.ANY)
     return pl.pallas_call(
         functools.partial(expert_kernel, n, capacity),
         name="expert_rows",
         out_shape=jax.ShapeDtypeStruct(came.shape, bf16),
-        in_specs=[VMEM_SPEC, any_spec, any_spec, any_spec],
+        in_specs=[VMEM_SPEC, any_spec, any_spec, any_spec, any_spec],
         out_specs=VMEM_SPEC,
         scratch_shapes=[
-            pltpu.VMEM(gate.shape, bf16),
+            pltpu.VMEM(up.shape, bf16),
             pltpu.VMEM(up.shape, bf16),
             pltpu.VMEM(down.shape, bf16),
             pltpu.VMEM((2 * BLOCK * capacity, width), bf16),
             pltpu.VMEM(came.shape, bf16),
-            pltpu.SemaphoreType.DMA((pieces, 3)),
+            pltpu.SemaphoreType.DMA((pieces, 4)),
             pltpu.SemaphoreType.DMA((n,)),
             pltpu.SemaphoreType.DMA((n,)),
         ],
         compiler_params=pltpu.CompilerParams(collective_id=number, has_side_effects=True),
         cost_estimate=pl.CostEstimate(flops=5 * 10**9, bytes_accessed=200 << 20, transcendentals=0),
-    )(came, gate, up, down)
+    )(came, early, gate, up, down)
 
 
 def combine_kernel(n, capacity, residual_ref, proj_ref, index_ref, weight_ref, back_ref, out_ref, rows_ref):
@@ -914,7 +1001,9 @@
         recept, key_input, value_input, decay_input_part, correction_rate_input, head_decay_offset,
         decay_fixed_bias[None], correction_rate_bias[None],
     )
-    enter = prefix_states(summary, n)
+    gate_shard = gate_weight_experts[0]
+    early_rows = gate_shard.shape[0] // 4
+    enter, early = prefix_states(summary, gate_shard, early_rows, n, lax.axis_size("tp"))
     down, enter = lax.optimization_barrier((down_weight_experts[0], enter))
     down = lax.all_gather(down, "tp")
     mixed = readout(
@@ -931,9 +1020,9 @@
     capacity = 3 * rows // experts
     outgoing = build(residual, proj, feedforward_norm_gain[None], routed_expert_index, experts, capacity)
     came, gate, up = exchange_and_gather(
-        outgoing, gate_weight_experts[0], up_weight_experts[0], n, lax.axis_size("tp"), 1
+        outgoing, gate_shard, up_weight_experts[0], early_rows, n, m, 1
     )
-    back = expert_rows(came, gate, up, down, capacity, 2)
+    back = expert_rows(came, early, gate, up, down, capacity, 2)
     return combine(residual, proj, routed_expert_index, routed_expert_weight, back, capacity)
 
 

time: 302 us -> 307 us (1.017)
  Pallas kernels: 277 us -> 282 us
  transfers between devices with their start and end apart: 2 -> 2, of which waited for: 0 -> 0; matrix products, arithmetic and copies ran while one was open for 3% -> 2% of each run, Pallas kernels for 62% -> 63%
where the time goes in v4:
time: 307 us; the launch traced here: 306 us
  Pallas kernels  282 us (92%)
  between operations  13.5 us (4%)
  local copies, waits for them, and re-layouts  5.77 us (2%)
  matrix products  4.56 us (1%)
    pallas_call x1, Pallas kernels, exchange_and_gather(): pl.pallas_call(functools.partial(exchange_gather_kernel, n, m, skip), nam...  101 us
    pallas_call x1, Pallas kernels, expert_rows(): pl.pallas_call(functools.partial(expert_kernel, n, capacity), name='exper...  86.3 us
    pallas_call x1, Pallas kernels, prefix_states(): pl.pallas_call(functools.partial(prefix_kernel, n, m, pairs), name='prefi...  44.3 us
    pallas_call x1, Pallas kernels, spread(): pl.pallas_call(functools.partial(spread_kernel, m), name='spread', out_sh...  17.4 us
    pallas_call x1, Pallas kernels, mixer_local(): pl.pallas_call(functools.partial(mixer_kernel, pairs, chunks), name='mixe...  16.9 us
  transfers between devices with their start and end apart: 2, of which 0 were waited for; matrix products, arithmetic and copies ran while one was open for 2% of the time, Pallas kernels for 63%

profile of v4, /device:TPU:33, one launch (start us, length us, event | category | flops | bytes accessed | tf_op | source)
XLA Modules:
  0.0 306.1 jit_solution(14328806861774727239)
XLA Ops:
  6.5 0.0 copy-start
  6.6 0.0 all-gather.5.cloned.1.call-start
  6.6 1.6 copy-done
  8.1 1.2 constant_dynamic-slice_fusion
  9.3 0.1 all-gather.5.cloned.1.call-update
  9.4 0.1 all-gather.7.cloned.1.call-start
  9.4 1.6 copy.20.offset_ref
  11.0 16.9 %mixer_local.1 = (bf16[4,2,64,128]{3,2,1,0:T(8,128)(2,1)}, bf16[512,512]{1,0:T(8,128)(2,1)}, f32[512,512]{1,0:T(8,128)}) custom-call(bf16[512,512]{1,0:T(8,128)(2,1)} %recept_ref.3, bf16[512,512]{1,0:T(8,128)(2,1)} %key_ref.3, bf16[512,512]{1,0:T(8,128)(2,1)} %value_ref.3, bf16[512,512]{1,0:T(8,128)(2,1)} %decay_ref.1, bf16[512,512]{1,0:T(8,128)(2,1)} %rate_ref.1, ...), custom_call_target="tpu_custom_call" | custom-call | flops 5368709120 | bytes 3145728 | tf_op jit(solution)/shard_map/mixer_local/pallas_call | solution.py:241
  27.9 0.0 copy-start.1
  27.9 0.0 copy-start.2
  27.9 44.3 %prefix_states.1 = (bf16[4,64,128]{2,1,0:T(8,128)(2,1)}, bf16[4,512,256]{2,1,0:T(8,128)(2,1)}) custom-call(bf16[4,2,64,128]{3,2,1,0:T(8,128)(2,1)} %get-tuple-element.17.summary_ref, bf16[2048,256]{1,0:T(8,128)(2,1)} %bitcast.21), custom_call_target="tpu_custom_call" | custom-call | flops 1000000000 | bytes 62914560 | tf_op jit(solution)/shard_map/prefix_states/pallas_call | solution.py:431
  72.2 0.1 all-gather.7.cloned.1.call-update
  72.3 0.0 copy-done.1
  72.3 0.7 copy.22.index_ref
  73.0 0.0 copy-done.2
  73.0 0.7 copy.23.weight_ref
  73.7 5.1 %readout.1 = bf16[512,512]{1,0:T(8,128)(2,1)} custom-call(bf16[512,512]{1,0:T(8,128)(2,1)} %recept_ref.3, bf16[512,512]{1,0:T(8,128)(2,1)} %key_ref.3, bf16[512,512]{1,0:T(8,128)(2,1)} %value_ref.3, bf16[512,512]{1,0:T(8,128)(2,1)} %gate_ref.1, f32[1,512]{1,0:T(1,128)} %bitcast.25, f32[1,512]{1,0:T(1,128)} %bitcast.26, ...), custom_call_target="tpu_custom_call" | custom-call | flops 1000000000 | bytes 16777216 | tf_op jit(solution)/shard_map/readout/pallas_call | solution.py:494
  78.8 17.4 %spread.1 = bf16[2,4,128,512]{3,2,1,0:T(8,128)(2,1)} custom-call(bf16[4,128,512]{2,1,0:T(8,128)(2,1)} %bitcast.20), custom_call_target="tpu_custom_call" | custom-call | flops 1000000 | bytes 41943040 | tf_op jit(solution)/shard_map/spread/pallas_call | solution.py:620
  96.2 0.0 all-gather.5.cloned.1.call-done
  96.3 4.6 %fusion.src_ref = bf16[2,128,1024]{2,1,0:T(8,128)(2,1)} fusion(bf16[2,4,128,512]{3,2,1,0:T(8,128)(2,1)} %spread.1, bf16[4,512,1024,1]{2,1,0,3:T(8,128)(2,1)} %bitcast.27), kind=kOutput, calls=%fused_computation.1 | convolution fusion | flops 1074003968 | bytes 5767168 | tf_op jit(solution)/shard_map/hjrc,jcd->hrd/dot_general | solution.py:1015
  100.8 3.4 %swap.1.proj_ref = bf16[2,128,1024]{2,1,0:T(8,128)(2,1)} custom-call(bf16[2,128,1024]{2,1,0:T(8,128)(2,1)} %fusion.src_ref), custom_call_target="tpu_custom_call" | custom-call | flops 1000000 | bytes 4194304 | tf_op jit(solution)/shard_map/swap/pallas_call | solution.py:654
  104.3 3.9 %build.1.src_ref = bf16[32,48,512]{2,1,0:T(8,128)(2,1)} custom-call(bf16[128,2048]{1,0:T(8,128)(2,1)} %residual_ref.3, bf16[2,128,1024]{2,1,0:T(8,128)(2,1)} %swap.1.proj_ref, f32[1,2048]{1,0:T(1,128)} %bitcast.29, s32[128,2]{1,0:T(8,128)} %copy.22.index_ref), custom_call_target="tpu_custom_call" | custom-call | flops 1000000000 | bytes 8388608 | tf_op jit(solution)/shard_map/build/pallas_call | solution.py:547
  108.1 100.8 %exchange_1.1 = (bf16[32,48,512]{2,1,0:T(8,128)(2,1)}, bf16[4,1536,256]{2,1,0:T(8,128)(2,1)}, bf16[4,2048,256]{2,1,0:T(8,128)(2,1)}) custom-call(bf16[32,48,512]{2,1,0:T(8,128)(2,1)} %build.1.src_ref, bf16[2048,256]{1,0:T(8,128)(2,1)} %bitcast.22, bf16[2048,256]{1,0:T(8,128)(2,1)} %bitcast.23), custom_call_target="tpu_custom_call" | custom-call | flops 1000000 | bytes 209715200 | tf_op jit(solution)/shard_map/exchange_1/pallas_call | solution.py:780
  209.0 0.0 all-gather.7.cloned.1.call-done
  209.0 86.3 %expert_rows.1.back_ref = bf16[32,48,512]{2,1,0:T(8,128)(2,1)} custom-call(bf16[32,48,512]{2,1,0:T(8,128)(2,1)} %get-tuple-element.20.came_ref, bf16[4,512,256]{2,1,0:T(8,128)(2,1)} %get-tuple-element.21.early_ref, bf16[4,1536,256]{2,1,0:T(8,128)(2,1)} %get-tuple-element.22.gate_ref, bf16[4,2048,256]{2,1,0:T(8,128)(2,1)} %get-tuple-element.23.up_ref, ...), custom_call_target="tpu_custom_call" | custom-call | flops 5000000000 | bytes 209715200 | tf_op jit(solution)/shard_map/expert_rows/pallas_call | solution.py:925
  295.3 4.0 %combine.1 = bf16[128,2048]{1,0:T(8,128)(2,1)} custom-call(bf16[128,2048]{1,0:T(8,128)(2,1)} %residual_ref.3, bf16[2,128,1024]{2,1,0:T(8,128)(2,1)} %swap.1.proj_ref, s32[128,2]{1,0:T(8,128)} %copy.22.index_ref, f32[128,2]{1,0:T(8,128)} %copy.23.weight_ref, bf16[32,48,512]{2,1,0:T(8,128)(2,1)} %expert_rows.1.back_ref), custom_call_target="tpu_custom_call" | custom-call | flops 1000000000 | bytes 8388608 | tf_op jit(solution)/shard_map/combine/pallas_call | solution.py:975
Async XLA Ops:
  6.5 1.6 copy-start
  6.6 89.7 %all-gather.5.cloned.1.call-start = ((), (), s32[]{:S(2)}) async-start(), calls=%async_computation | async-start | bytes 5242880 | tf_op jit(solution)/shard_map/all_gather | solution.py:998
  9.4 199.6 %all-gather.7.cloned.1.call-start = ((), (), s32[]{:S(2)}) async-start(), calls=%async_computation.1 | async-start | bytes 5242880 | tf_op jit(solution)/shard_map/all_gather | solution.py:1008
  27.9 44.4 %copy-start.1 = (s32[128,2]{0,1:T(2,128)S(1)}, s32[128,2]{0,1:T(2,128)}, u32[]{:S(2)}) copy-start(s32[128,2]{0,1:T(2,128)} %param.33) | copy-start | bytes 3076
  27.9 45.1 %copy-start.2 = (f32[128,2]{0,1:T(2,128)S(1)}, f32[128,2]{0,1:T(2,128)}, u32[]{:S(2)}) copy-start(f32[128,2]{0,1:T(2,128)} %param.34) | copy-start | bytes 3076
Sparse Core Ops, SparseCore 0:
  9.5 77.1 all-gather.4
  88.5 85.5 all-gather.6

commit v5 on v3

--- a/solution.py
+++ b/solution.py
@@ -762,7 +762,6 @@
     gather_order, spread_order = reorder(capacity, True), reorder(capacity, False)
     for load in loads:
         load.wait()
-    pl.semaphore_wait(barrier, n - 1)
 
     def home(device):
         return pltpu.make_async_remote_copy(
@@ -807,6 +806,10 @@
                 def _():
                     out_ref[me] = result
 
+        @pl.when(c == 0)
+        def _():
+            pl.semaphore_wait(barrier, n - 1)
+
         for g in both:
             for k in range(BLOCK):
                 device = g * BLOCK + k

time: 302 us -> 299 us (0.990)
  transfers between devices with their start and end apart: 2 -> 2, of which waited for: 0 -> 0; matrix products, arithmetic and copies ran while one was open for 3% -> 3% of each run, Pallas kernels for 62% -> 63%
where the time goes in v5:
time: 299 us
  Pallas kernels  275 us (92%)
  between operations  13.5 us (5%)
  local copies, waits for them, and re-layouts  5.78 us (2%)
  matrix products  4.56 us (2%)
    pallas_call x1, Pallas kernels, exchange_and_gather(): pl.pallas_call(functools.partial(exchange_gather_kernel, n, m), name=f'ex...  102 us
    pallas_call x1, Pallas kernels, expert_rows(): pl.pallas_call(functools.partial(expert_kernel, n, capacity), name='exper...  83.8 us
    pallas_call x1, Pallas kernels, prefix_states(): pl.pallas_call(functools.partial(prefix_kernel, n, pairs), name='prefix_s...  40.9 us
    pallas_call x1, Pallas kernels, mixer_local(): pl.pallas_call(functools.partial(mixer_kernel, pairs, chunks), name='mixe...  16.9 us
    pallas_call x1, Pallas kernels, spread(): pl.pallas_call(functools.partial(spread_kernel, m), name='spread', out_sh...  15.2 us
  transfers between devices with their start and end apart: 2, of which 0 were waited for; matrix products, arithmetic and copies ran while one was open for 3% of the time, Pallas kernels for 63%

profile of v5, /device:TPU:33, one launch (start us, length us, event | category | flops | bytes accessed | tf_op | source)
XLA Modules:
  0.0 298.8 jit_solution(16411441904865445204)
XLA Ops:
  6.5 0.0 copy-start
  6.6 0.0 all-gather.5.cloned.1.call-start
  6.6 1.6 copy-done
  8.1 1.2 constant_dynamic-slice_fusion
  9.3 0.1 all-gather.5.cloned.1.call-update
  9.4 0.1 all-gather.7.cloned.1.call-start
  9.4 1.6 copy.20.offset_ref
  11.0 16.9 %mixer_local.1 = (bf16[4,2,64,128]{3,2,1,0:T(8,128)(2,1)}, bf16[512,512]{1,0:T(8,128)(2,1)}, f32[512,512]{1,0:T(8,128)}) custom-call(bf16[512,512]{1,0:T(8,128)(2,1)} %recept_ref.3, bf16[512,512]{1,0:T(8,128)(2,1)} %key_ref.3, bf16[512,512]{1,0:T(8,128)(2,1)} %value_ref.3, bf16[512,512]{1,0:T(8,128)(2,1)} %decay_ref.1, bf16[512,512]{1,0:T(8,128)(2,1)} %rate_ref.1, ...), custom_call_target="tpu_custom_call" | custom-call | flops 5368709120 | bytes 3145728 | tf_op jit(solution)/shard_map/mixer_local/pallas_call | solution.py:241
  27.9 0.0 copy-start.1
  27.9 0.0 copy-start.2
  27.9 40.9 %prefix_states.1.enter_ref = bf16[4,64,128]{2,1,0:T(8,128)(2,1)} custom-call(bf16[4,2,64,128]{3,2,1,0:T(8,128)(2,1)} %get-tuple-element.15.summary_ref), custom_call_target="tpu_custom_call" | custom-call | flops 1000000000 | bytes 62914560 | tf_op jit(solution)/shard_map/prefix_states/pallas_call | solution.py:366
  68.8 0.1 all-gather.7.cloned.1.call-update
  68.9 0.0 copy-done.1
  68.9 0.7 copy.22.index_ref
  69.6 0.0 copy-done.2
  69.6 0.7 copy.23.weight_ref
  70.4 5.1 %readout.1 = bf16[512,512]{1,0:T(8,128)(2,1)} custom-call(bf16[512,512]{1,0:T(8,128)(2,1)} %recept_ref.3, bf16[512,512]{1,0:T(8,128)(2,1)} %key_ref.3, bf16[512,512]{1,0:T(8,128)(2,1)} %value_ref.3, bf16[512,512]{1,0:T(8,128)(2,1)} %gate_ref.1, f32[1,512]{1,0:T(1,128)} %bitcast.24, f32[1,512]{1,0:T(1,128)} %bitcast.25, ...), custom_call_target="tpu_custom_call" | custom-call | flops 1000000000 | bytes 16777216 | tf_op jit(solution)/shard_map/readout/pallas_call | solution.py:419
  75.4 15.2 %spread.1 = bf16[2,4,128,512]{3,2,1,0:T(8,128)(2,1)} custom-call(bf16[4,128,512]{2,1,0:T(8,128)(2,1)} %bitcast.20), custom_call_target="tpu_custom_call" | custom-call | flops 1000000 | bytes 41943040 | tf_op jit(solution)/shard_map/spread/pallas_call | solution.py:545
  90.7 0.0 all-gather.5.cloned.1.call-done
  90.7 4.6 %fusion.src_ref = bf16[2,128,1024]{2,1,0:T(8,128)(2,1)} fusion(bf16[2,4,128,512]{3,2,1,0:T(8,128)(2,1)} %spread.1, bf16[4,512,1024,1]{2,1,0,3:T(8,128)(2,1)} %bitcast.26), kind=kOutput, calls=%fused_computation.1 | convolution fusion | flops 1074003968 | bytes 5767168 | tf_op jit(solution)/shard_map/hjrc,jcd->hrd/dot_general | solution.py:929
  95.3 3.5 %swap.1.proj_ref = bf16[2,128,1024]{2,1,0:T(8,128)(2,1)} custom-call(bf16[2,128,1024]{2,1,0:T(8,128)(2,1)} %fusion.src_ref), custom_call_target="tpu_custom_call" | custom-call | flops 1000000 | bytes 4194304 | tf_op jit(solution)/shard_map/swap/pallas_call | solution.py:579
  98.7 3.9 %build.1.src_ref = bf16[32,48,512]{2,1,0:T(8,128)(2,1)} custom-call(bf16[128,2048]{1,0:T(8,128)(2,1)} %residual_ref.3, bf16[2,128,1024]{2,1,0:T(8,128)(2,1)} %swap.1.proj_ref, f32[1,2048]{1,0:T(1,128)} %bitcast.28, s32[128,2]{1,0:T(8,128)} %copy.22.index_ref), custom_call_target="tpu_custom_call" | custom-call | flops 1000000000 | bytes 8388608 | tf_op jit(solution)/shard_map/build/pallas_call | solution.py:472
  102.6 101.5 %exchange_1.1 = (bf16[32,48,512]{2,1,0:T(8,128)(2,1)}, bf16[4,2048,256]{2,1,0:T(8,128)(2,1)}, bf16[4,2048,256]{2,1,0:T(8,128)(2,1)}) custom-call(bf16[32,48,512]{2,1,0:T(8,128)(2,1)} %build.1.src_ref, bf16[2048,256]{1,0:T(8,128)(2,1)} %bitcast.21, bf16[2048,256]{1,0:T(8,128)(2,1)} %bitcast.22), custom_call_target="tpu_custom_call" | custom-call | flops 1000000 | bytes 209715200 | tf_op jit(solution)/shard_map/exchange_1/pallas_call | solution.py:705
  204.2 0.0 all-gather.7.cloned.1.call-done
  204.2 83.8 %expert_rows.1.back_ref = bf16[32,48,512]{2,1,0:T(8,128)(2,1)} custom-call(bf16[32,48,512]{2,1,0:T(8,128)(2,1)} %get-tuple-element.17.came_ref, bf16[4,2048,256]{2,1,0:T(8,128)(2,1)} %get-tuple-element.18.gate_ref, bf16[4,2048,256]{2,1,0:T(8,128)(2,1)} %get-tuple-element.19.up_ref, bf16[4,256,2048]{2,1,0:T(8,128)(2,1)} %bitcast.27), custom_call_target="tpu_custom_call" | custom-call | flops 5000000000 | bytes 209715200 | tf_op jit(solution)/shard_map/expert_rows/pallas_call | solution.py:841
  288.0 4.0 %combine.1 = bf16[128,2048]{1,0:T(8,128)(2,1)} custom-call(bf16[128,2048]{1,0:T(8,128)(2,1)} %residual_ref.3, bf16[2,128,1024]{2,1,0:T(8,128)(2,1)} %swap.1.proj_ref, s32[128,2]{1,0:T(8,128)} %copy.22.index_ref, f32[128,2]{1,0:T(8,128)} %copy.23.weight_ref, bf16[32,48,512]{2,1,0:T(8,128)(2,1)} %expert_rows.1.back_ref), custom_call_target="tpu_custom_call" | custom-call | flops 1000000000 | bytes 8388608 | tf_op jit(solution)/shard_map/combine/pallas_call | solution.py:891
Async XLA Ops:
  6.5 1.6 copy-start
  6.6 84.1 %all-gather.5.cloned.1.call-start = ((), (), s32[]{:S(2)}) async-start(), calls=%async_computation | async-start | bytes 5242880 | tf_op jit(solution)/shard_map/all_gather | solution.py:914
  9.4 194.8 %all-gather.7.cloned.1.call-start = ((), (), s32[]{:S(2)}) async-start(), calls=%async_computation.1 | async-start | bytes 5242880 | tf_op jit(solution)/shard_map/all_gather | solution.py:922
  27.9 41.0 %copy-start.1 = (s32[128,2]{0,1:T(2,128)S(1)}, s32[128,2]{0,1:T(2,128)}, u32[]{:S(2)}) copy-start(s32[128,2]{0,1:T(2,128)} %param.33) | copy-start | bytes 3076
  27.9 41.7 %copy-start.2 = (f32[128,2]{0,1:T(2,128)S(1)}, f32[128,2]{0,1:T(2,128)}, u32[]{:S(2)}) copy-start(f32[128,2]{0,1:T(2,128)} %param.34) | copy-start | bytes 3076
Sparse Core Ops, SparseCore 0:
  9.5 68.6 all-gather.4
  80.0 71.8 all-gather.6
